TPU v7x, 32 devices: a whole 2x2x4 slice. The times are simulated.
32 devices in a mesh: sp: 16 (over z, y, x), tp: 2 (over core).
Axes of the slice: x: 2, y: 2, z: 4, core: 2. Of those that a mesh axis runs over, the one named last changes fastest.
Arguments:
- prompt: bfloat16 [16, 1024, 2048], P('sp', None, 'tp'), may hold values from -6 to 6
- new_input: bfloat16 [16, 2048], P('sp', 'tp'), may hold values from -140 to 140
- w_query: bfloat16 [2048, 2048], P('sp', 'tp'), may hold values from -0.21875 to 0.21875
- w_key: bfloat16 [2048, 2048], P('sp', 'tp'), may hold values from -0.125 to 0.125
- w_value: bfloat16 [2048, 2048], P('sp', 'tp'), may hold values from -0.125 to 0.125
- lam: float32 [16], P('tp'), may hold values from 0.3 to 0.8
- out_gain: float32 [128], replicated, may hold values from 0.1 to 1.9
Outputs:
- key_cache: bfloat16 [16, 1024, 2048], P('sp', None, 'tp')
- value_cache: bfloat16 [16, 1024, 2048], P('sp', None, 'tp')
- first_read: bfloat16 [16, 16, 128], P('sp', 'tp')
All inputs are finite; a program needn't handle non-finite values.
Results may differ from a plain program's by a relative error of at most 0.02.
The roundings to bfloat16 on the way count: a program that leaves them out, or rounds other values in their place, can miss the bound.
Values may be sent and summed in bfloat16 or wider, within the bound.
A program may use at most 64 MiB of HBM per device.

v0:
```python
import functools

import jax
import jax.numpy as jnp
from jax import lax
from jax.experimental import pallas as pl
from jax.experimental.pallas import tpu as pltpu
from jax.sharding import PartitionSpec as P

MAP_DIM = 64
VAL_DIM = 128
LANES = 128
rope_base = 500000.0
norm_eps = 1e-05

X, Y, UP, DOWN = 0, 1, 2, 3
F32, BF16 = jnp.float32, jnp.bfloat16


def inverse_freq():
    return rope_base ** (-(jnp.arange(MAP_DIM // 2, dtype=F32) * 2.0 / MAP_DIM))


def table(position, inverse):
    angle = position * inverse
    lane = lax.broadcasted_iota(jnp.int32, angle.shape, 1) % MAP_DIM
    sine = jnp.sin(angle)
    return jnp.cos(angle), jnp.where(lane < MAP_DIM // 2, -sine, sine)


def rotated(tile, cosine, sine):
    half = MAP_DIM // 2
    lane = lax.broadcasted_iota(jnp.int32, tile.shape, 1) % MAP_DIM
    other = jnp.where(lane < half, pltpu.roll(tile, LANES - half, 1), pltpu.roll(tile, half, 1))
    return tile * cosine + other * sine


def kernel(
    n, tp, prompt, fresh, wq, wk, wv, inverse,
    k_out, v_out, q_out,
    W, PR, acc, ko, vo, fr, XN, XM, wq_v, QS, QR, ct, st,
    w_recv, w_send, p_recv, p_send, x_recv, x_send, xt_recv, xt_send, q_recv, q_send, loc, token,
):
    _, rows, wl = prompt.shape
    depth, cols = wk.shape
    half = cols // 2
    heads = cols // VAL_DIM
    L = n // 4
    plane = 4 * depth
    me, mt = lax.axis_index("sp"), lax.axis_index("tp")
    z, y, x = me // 4, (me // 2) % 2, me % 2
    yf, xf = 1 - y, 1 - x

    def at(zo, yo, xo):
        return zo * 4 + yo * 2 + xo

    partner = {X: at(z, y, xf), Y: at(z, yf, x), UP: me + 4, DOWN: me - 4}

    def piece(c, o):
        return W.at[c, pl.ds(pl.multiple_of(o * depth, depth), depth), :]

    def copy(c, d, o):
        return pltpu.make_async_remote_copy(
            src_ref=piece(c, o), dst_ref=piece(c, o),
            send_sem=w_send.at[(c * 4 + d) * n + o], recv_sem=w_recv.at[c * n + o],
            device_id={"sp": partner[d]}, device_id_type=pl.DeviceIdType.MESH,
        )

    def send(c, d, o):
        copy(c, d, o).start()

    def got(c, o):
        copy(c, X, o).wait_recv()

    barrier = pltpu.get_barrier_semaphore()
    for d in range(1, tp):
        pl.semaphore_signal(
            barrier, inc=1, device_id={"tp": (mt + d) % tp}, device_id_type=pl.DeviceIdType.MESH)

    up_ok, down_ok = z + 1 < L, z > 0

    def signal(sem, d):
        pl.semaphore_signal(
            sem, inc=1, device_id={"sp": partner[d]}, device_id_type=pl.DeviceIdType.MESH)

    signal(barrier, X)
    signal(barrier, Y)
    pl.when(up_ok)(lambda: signal(barrier, UP))
    pl.when(down_ok)(lambda: signal(barrier, DOWN))

    def columns(t):
        return PR.at[:, pl.ds(pl.multiple_of(t * wl, wl), wl)]

    own = [
        pltpu.make_async_copy(w.at[:, pl.ds(h * half, half)], piece(2 * i + h, me), loc.at[2 * i + h])
        for i, w in enumerate((wk, wv)) for h in range(2)
    ]
    rest = [
        pltpu.make_async_copy(fresh, fr, loc.at[4]),
        pltpu.make_async_copy(prompt.at[0], columns(mt), loc.at[5]),
        pltpu.make_async_copy(wq, wq_v, loc.at[6]),
    ]
    rest[0].start()
    for c in own:
        c.start()
    for c in rest[1:]:
        c.start()
    rest[0].wait()
    XN[mt, me] = fr[...].astype(F32)
    for c in own:
        c.wait()

    @pl.when(up_ok & down_ok)
    def _():
        pl.semaphore_wait(barrier, 4 + tp - 1)

    @pl.when(jnp.logical_not(up_ok & down_ok))
    def _():
        pl.semaphore_wait(barrier, 3 + tp - 1)

    def x_copy(d):
        return pltpu.make_async_remote_copy(
            src_ref=XN.at[mt, me], dst_ref=XN.at[mt, me],
            send_sem=x_send.at[d], recv_sem=x_recv.at[me],
            device_id={"sp": (me + d) % n}, device_id_type=pl.DeviceIdType.MESH,
        )

    def x_wait(d):
        src = (me + d) % n
        return pltpu.make_async_remote_copy(
            src_ref=XN.at[mt, src], dst_ref=XN.at[mt, src],
            send_sem=x_send.at[d], recv_sem=x_recv.at[src],
            device_id={"sp": src}, device_id_type=pl.DeviceIdType.MESH,
        )

    def loop(lo, hi, f):
        lax.fori_loop(lo, hi, lambda i, _: (f(i), _)[1], 0)

    def along_z(c, o):
        @pl.when(up_ok)
        def _():
            send(c, UP, o)

        @pl.when(down_ok)
        def _():
            send(c, DOWN, o)

    send(0, Y, me)
    send(1, X, me)
    along_z(2, me)
    along_z(3, me)
    send(2, X, me)
    send(3, Y, me)

    signal(token.at[Y], Y)

    pl.semaphore_wait(token.at[Y], 1)
    signal(token.at[X], X)
    pl.semaphore_wait(token.at[X], 1)
    for ok, more, d in ((down_ok, up_ok, UP), (up_ok, down_ok, DOWN)):
        @pl.when(ok)
        def _(d=d):
            pl.semaphore_wait(token.at[d], 1)

        @pl.when(more)
        def _(d=d):
            signal(token.at[d], d)
    loop(1, n, lambda d: x_copy(d).start())

    along_z(0, me)
    along_z(1, me)
    send(0, X, me)
    send(1, Y, me)
    send(2, Y, me)
    send(3, X, me)

    def p_copy(d):
        return pltpu.make_async_remote_copy(
            src_ref=prompt.at[0], dst_ref=columns(mt),
            send_sem=p_send.at[d], recv_sem=p_recv.at[mt],
            device_id={"tp": (mt + d) % tp}, device_id_type=pl.DeviceIdType.MESH,
        )

    def p_wait(d):
        src = (mt + d) % tp
        return pltpu.make_async_remote_copy(
            src_ref=columns(src), dst_ref=columns(src),
            send_sem=p_send.at[d], recv_sem=p_recv.at[src],
            device_id={"tp": src}, device_id_type=pl.DeviceIdType.MESH,
        )

    for d in range(1, tp):
        p_copy(d).start()

    o_y, o_x = at(z, yf, x), at(z, y, xf)
    got(0, o_y)
    along_z(0, o_y)
    send(0, X, o_y)
    got(1, o_x)
    along_z(1, o_x)
    send(1, Y, o_x)

    got(2, o_x)
    send(2, Y, o_x)
    got(3, o_y)
    send(3, X, o_y)

    rest[1].wait()
    for d in range(1, tp):
        p_wait(d).wait_recv()

    def relay(s):
        sides = ((z - s, z - s >= 0, up_ok, UP), (z + s, z + s < L, down_ok, DOWN))

        def along(c, yo, xo, across):
            for zo, valid, more, d in sides:
                @pl.when(valid)
                def _(zo=zo, more=more, d=d):
                    o = at(zo, yo, xo)
                    got(c, o)

                    @pl.when(more)
                    def _():
                        send(c, d, o)

                    for a in across:
                        send(c, a, o)

        along(2, y, x, (X, Y))
        along(3, y, x, (Y, X))
        along(0, y, x, (X,))
        along(1, y, x, (Y,))
        for zo, valid, _, _ in sides:
            @pl.when(valid)
            def _(zo=zo):
                got(2, at(zo, y, xf))
                send(2, Y, at(zo, y, xf))
                got(3, at(zo, yf, x))
                send(3, X, at(zo, yf, x))
        along(0, yf, x, (X,))
        along(1, y, xf, (Y,))

    R = min(rows, 256)

    def dots(zo):
        for c, order in ((2, ((yf, x), (yf, xf))), (3, ((y, xf), (yf, xf))),
                         (0, ((y, xf), (yf, xf))), (1, ((yf, x), (yf, xf)))):
            for yo, xo in order:
                got(c, at(zo, yo, xo))

            def tile(i, c=c):
                r = pl.ds(pl.multiple_of(i * R, R), R)
                p = pl.ds(pl.multiple_of(zo * plane, plane), plane)
                acc[c, r, :] += jnp.dot(PR[r, p], W[c, p, :], preferred_element_type=F32)

            loop(0, rows // R, tile)

    def finish(s):
        @pl.when(z - s >= 0)
        def _():
            dots(z - s)

        @pl.when((z + s < L) & (s > 0))
        def _():
            dots(z + s)

    if L > 1:
        relay(1)

    loop(1, n, lambda d: x_wait(d).wait_recv())

    def xt_copy(d, t):
        return pltpu.make_async_remote_copy(
            src_ref=XN.at[t], dst_ref=XN.at[t],
            send_sem=xt_send.at[d], recv_sem=xt_recv.at[t],
            device_id={"tp": (mt + d) % tp}, device_id_type=pl.DeviceIdType.MESH,
        )

    for d in range(1, tp):
        xt_copy(d, mt).start()
    for d in range(1, tp):
        xt_copy(d, (mt + d) % tp).wait_recv()
    first = me * depth
    holder, offset = first // wl, first % wl
    for j in range(n):
        XM[pl.ds(j, 1), :] = XN[holder, j]
    pick = (
        lax.broadcasted_iota(jnp.int32, (wl, depth), 0)
        == offset + lax.broadcasted_iota(jnp.int32, (wl, depth), 1)
    )
    chosen = jnp.dot(
        XM[...].astype(BF16), jnp.where(pick, 1.0, 0.0).astype(BF16), preferred_element_type=F32
    ).astype(BF16)
    rest[2].wait()
    partial = jnp.dot(chosen, wq_v[...], preferred_element_type=F32)
    for j in range(n):
        QS[j] = partial[j:j + 1, :]
    QR[me] = QS[me]

    def zero(i):
        acc[i // (rows // 128), pl.ds(pl.multiple_of((i % (rows // 128)) * 128, 128), 128), :] = (
            jnp.zeros((128, half), F32))

    loop(0, 4 * (rows // 128), zero)

    def angles(i):
        position = (i * 64 + lax.broadcasted_iota(jnp.int32, (64, LANES), 0)).astype(F32)
        r = pl.ds(pl.multiple_of(i * 64, 64), 64)
        ct[r, :], st[r, :] = table(position, inverse[...])

    loop(0, rows // 64, angles)
    qcos, qsin = table(jnp.full((8, LANES), rows, F32), inverse[...])

    def q_copy(d):
        dst = (me + d) % n
        return pltpu.make_async_remote_copy(
            src_ref=QS.at[dst], dst_ref=QR.at[me],
            send_sem=q_send.at[d], recv_sem=q_recv.at[me],
            device_id={"sp": dst}, device_id_type=pl.DeviceIdType.MESH,
        )

    def q_wait(d):
        src = (me + d) % n
        return pltpu.make_async_remote_copy(
            src_ref=QS.at[src], dst_ref=QR.at[src],
            send_sem=q_send.at[d], recv_sem=q_recv.at[src],
            device_id={"sp": src}, device_id_type=pl.DeviceIdType.MESH,
        )

    loop(1, n, lambda d: q_copy(d).start())

    finish(0)

    def step(s):
        relay(s)
        finish(s - 1)

    loop(2, L, step)

    loop(1, n, lambda d: q_wait(d).wait_recv())
    total = QR[0]
    for j in range(1, n):
        total = total + QR[j]
    total = jnp.broadcast_to(total, (8, cols))
    query = jnp.concatenate(
        [rotated(total[:, i:i + LANES], qcos, qsin) for i in range(0, cols, LANES)], axis=1)
    maps = 2 * heads
    pad = max(maps, 16)
    query = jnp.broadcast_to(query[:1], (pad, cols))
    keep = (
        lax.broadcasted_iota(jnp.int32, (pad, cols), 0)
        == lax.broadcasted_iota(jnp.int32, (pad, cols), 1) // MAP_DIM
    )
    q_out[...] = jnp.where(keep, query, 0.0).astype(BF16)

    if L > 1:
        finish(L - 1)

    def rotate_rows(i):
        r = pl.ds(pl.multiple_of(i * R, R), R)
        cosine, sine = ct[r, :], st[r, :]
        for j in range(0, cols, LANES):
            tile = acc[j // half, r, pl.ds(j % half, LANES)]
            ko[r, pl.ds(j, LANES)] = rotated(tile, cosine, sine).astype(BF16)

    def value_rows(i):
        r = pl.ds(pl.multiple_of(i * R, R), R)
        for h in range(2):
            vo[r, pl.ds(h * half, half)] = acc[2 + h, r, :].astype(BF16)

    v_copy = pltpu.make_async_copy(vo, v_out.at[0], loc.at[1])
    k_copy = pltpu.make_async_copy(ko, k_out.at[0], loc.at[0])
    loop(0, rows // R, value_rows)
    v_copy.start()
    loop(0, rows // R, rotate_rows)
    k_copy.start()

    loop(1, n, lambda d: x_copy(d).wait_send())
    loop(1, n, lambda d: q_copy(d).wait_send())
    for d in range(1, tp):
        p_copy(d).wait_send()
        xt_copy(d, mt).wait_send()
    copy(0, Y, me).wait_send()
    copy(1, X, me).wait_send()

    def sent(zo):
        a, ay, ax = at(zo, y, x), at(zo, yf, x), at(zo, y, xf)
        for c, o in ((0, a), (0, ay), (2, a), (3, a), (3, ay)):
            copy(c, X, o).wait_send()
        for c, o in ((1, a), (1, ax), (3, a), (2, a), (2, ax)):
            copy(c, Y, o).wait_send()
        for ok, d in ((up_ok & (zo <= z), UP), (down_ok & (zo >= z), DOWN)):
            @pl.when(ok)
            def _(d=d):
                for c, o in ((0, a), (0, ay), (1, a), (1, ax), (2, a), (3, a)):
                    copy(c, d, o).wait_send()

    loop(0, L, sent)
    v_copy.wait()
    k_copy.wait()


def read(keys, values, query, lam, gain, k_out, v_out, read_out, ko, vo, sem):
    heads, pad = lam.shape[0], query.shape[0]
    v_in = pltpu.make_async_copy(values.at[0], vo, sem.at[1])
    k_in = pltpu.make_async_copy(keys.at[0], ko, sem.at[0])
    k_copy = pltpu.make_async_copy(ko, k_out.at[0], sem.at[2])
    v_copy = pltpu.make_async_copy(vo, v_out.at[0], sem.at[3])
    k_in.start()
    v_in.start()
    k_in.wait()
    k_copy.start()
    scores = lax.dot_general(
        query[...], ko[...], (((1,), (1,)), ((), ())), preferred_element_type=F32) * MAP_DIM ** -0.5
    weights = jnp.exp(scores - jnp.max(scores, axis=-1, keepdims=True))
    weights = weights / jnp.sum(weights, axis=-1, keepdims=True)
    high = weights.astype(BF16)
    left = weights - high.astype(F32)
    mid = left.astype(BF16)
    low = (left - mid.astype(F32)).astype(BF16)
    v_in.wait()
    v_copy.start()
    mixed = jnp.dot(jnp.concatenate([high, mid, low], axis=0), vo[...], preferred_element_type=F32)
    mixed = mixed[:pad] + mixed[pad:2 * pad] + mixed[2 * pad:]
    reads = []
    for h in range(heads):
        c = slice(h * VAL_DIM, (h + 1) * VAL_DIM)
        diff = mixed[2 * h:2 * h + 1, c] - lam[h] * mixed[2 * h + 1:2 * h + 2, c]
        normed = diff * lax.rsqrt(jnp.mean(diff * diff, axis=-1, keepdims=True) + norm_eps)
        reads.append(normed * gain[...])
    read_out[0] = jnp.concatenate(reads, axis=0).astype(BF16)
    k_copy.wait()
    v_copy.wait()


def body(n, tp, prompt, new_input, w_query, w_key, w_value, lam, out_gain):
    seqs, rows, wl = prompt.shape
    depth, cols = w_key.shape
    heads = lam.shape[0]
    half = cols // 2
    pad = max(2 * heads, 16)
    inverse = jnp.tile(inverse_freq(), LANES * 2 // MAP_DIM)[None, :]
    any_ = pl.BlockSpec(memory_space=pl.ANY)
    hbm = pl.BlockSpec(memory_space=pltpu.HBM)
    vmem = pl.BlockSpec(memory_space=pltpu.VMEM)
    smem = pl.BlockSpec(memory_space=pltpu.SMEM)
    dma = pltpu.SemaphoreType.DMA
    keys, values, query = pl.pallas_call(
        functools.partial(kernel, n, tp),
        out_shape=(
            jax.ShapeDtypeStruct((seqs, rows, cols), BF16),
            jax.ShapeDtypeStruct((seqs, rows, cols), BF16),
            jax.ShapeDtypeStruct((pad, cols), BF16),
        ),
        in_specs=[hbm] * 5 + [vmem],
        out_specs=(any_, any_, vmem),
        scratch_shapes=[
            pltpu.VMEM((4, n * depth, half), BF16),
            pltpu.VMEM((rows, tp * wl), BF16),
            pltpu.VMEM((4, rows, half), F32),
            pltpu.VMEM((rows, cols), BF16),
            pltpu.VMEM((rows, cols), BF16),
            pltpu.VMEM((1, wl), BF16),
            pltpu.VMEM((tp, n, 1, wl), F32),
            pltpu.VMEM((n, wl), F32),
            pltpu.VMEM((depth, cols), BF16),
            pltpu.VMEM((n, 1, cols), F32),
            pltpu.VMEM((n, 1, cols), F32),
            pltpu.VMEM((rows, LANES), F32),
            pltpu.VMEM((rows, LANES), F32),
            dma((4 * n,)), dma((16 * n,)), dma((tp,)), dma((tp,)), dma((n,)), dma((n,)),
            dma((tp,)), dma((tp,)), dma((n,)), dma((n,)), dma((7,)), pltpu.SemaphoreType.REGULAR((4,)),
        ],
        compiler_params=pltpu.CompilerParams(
            collective_id=0, has_side_effects=True, vmem_limit_bytes=56 * 1024 * 1024),
        name="prefill",
    )(prompt, new_input, w_query, w_key, w_value, inverse)
    return pl.pallas_call(
        read,
        out_shape=(
            jax.ShapeDtypeStruct((seqs, rows, cols), BF16),
            jax.ShapeDtypeStruct((seqs, rows, cols), BF16),
            jax.ShapeDtypeStruct((seqs, heads, VAL_DIM), BF16),
        ),
        in_specs=[any_, any_, vmem, smem, vmem],
        out_specs=(any_, any_, vmem),
        scratch_shapes=[pltpu.VMEM((rows, cols), BF16), pltpu.VMEM((rows, cols), BF16), dma((4,))],
        compiler_params=pltpu.CompilerParams(vmem_limit_bytes=56 * 1024 * 1024),
        name="read",
    )(keys, values, query, lam, out_gain[None, :])


def solution(mesh):
    in_specs = (
        P("sp", None, "tp"), P("sp", "tp"), P("sp", "tp"), P("sp", "tp"), P("sp", "tp"), P("tp"), P(),
    )
    out_specs = (P("sp", None, "tp"), P("sp", None, "tp"), P("sp", "tp", None))
    return jax.shard_map(
        functools.partial(body, mesh.shape["sp"], mesh.shape["tp"]),
        mesh=mesh, in_specs=in_specs, out_specs=out_specs, check_vma=False)
```

profile of v0, /device:TPU:0, one launch (start us, length us, event | category | flops | bytes accessed | tf_op | source)
XLA Modules:
  0.0 90.2 jit_solution(17217253756881993422)
XLA Ops:
  0.7 0.6 broadcast_in_dim_tile.3.inverse
  1.2 83.7 %prefill.1 = (bf16[1,1024,1024]{2,1,0:T(8,128)(2,1)}, bf16[1,1024,1024]{2,1,0:T(8,128)(2,1)}, bf16[16,1024]{1,0:T(8,128)(2,1)}) custom-call(bf16[1,1024,1024]{2,1,0:T(8,128)(2,1)} %prompt.1, bf16[1,1024]{1,0:T(2,128)(2,1)} %fresh.1, bf16[128,1024]{1,0:T(8,128)(2,1)} %wq.1, bf16[128,1024]{1,0:T(8,128)(2,1)} %wk.1, bf16[128,1024]{1,0:T(8,128)(2,1)} %wv.1, ...), custom_call_target="tpu_custom_call" | custom-call | tf_op jit(solution)/shard_map/prefill/pallas_call | solution.py:448
  85.0 5.2 %read.1 = (bf16[1,1024,1024]{2,1,0:T(8,128)(2,1)}, bf16[1,1024,1024]{2,1,0:T(8,128)(2,1)}, bf16[1,8,128]{2,1,0:T(8,128)(2,1)}) custom-call(bf16[1,1024,1024]{2,1,0:T(8,128)(2,1)} %get-tuple-element.6.keys, bf16[1,1024,1024]{2,1,0:T(8,128)(2,1)} %get-tuple-element.7.values, bf16[16,1024]{1,0:T(8,128)(2,1)} %get-tuple-element.8.query, f32[8]{0:T(128)} %lam.1, ...), custom_call_target="tpu_custom_call" | custom-call | tf_op jit(solution)/shard_map/read/pallas_call | solution.py:478
  (2 shorter events, 0.0 us)
where the time goes:
time: 90.4 us; the launch traced here: 90.2 us
  Pallas kernels  88.9 us (98%)
    pallas_call x1, Pallas kernels, body(): pl.pallas_call(functools.partial(kernel, n, tp), out_shape=(jax.ShapeDtyp...  83.7 us
    pallas_call x1, Pallas kernels, body(): pl.pallas_call(read, out_shape=(jax.ShapeDtypeStruct((seqs, rows, cols),...  5.17 us

commit v1 on v0

v1 whole, which is shorter than its diff:
```python
import functools
import math

import jax
import jax.numpy as jnp
from jax import lax
from jax.experimental import pallas as pl
from jax.experimental.pallas import tpu as pltpu
from jax.sharding import PartitionSpec as P

MAP_DIM = 64
VAL_DIM = 128
LANES = 128
rope_base = 500000.0
norm_eps = 1e-05

X, Y, UP, DOWN = 0, 1, 2, 3
F32, BF16 = jnp.float32, jnp.bfloat16


def inverse_freq(shape):
    lane = lax.broadcasted_iota(jnp.int32, shape, 1) % (MAP_DIM // 2)
    return jnp.exp(lane.astype(F32) * (-2.0 / MAP_DIM * math.log(rope_base)))


def table(position):
    angle = position * inverse_freq(position.shape)
    lane = lax.broadcasted_iota(jnp.int32, angle.shape, 1) % MAP_DIM
    sine = jnp.sin(angle)
    return jnp.cos(angle), jnp.where(lane < MAP_DIM // 2, -sine, sine)


def rotated(tile, cosine, sine):
    half = MAP_DIM // 2
    lane = lax.broadcasted_iota(jnp.int32, tile.shape, 1) % MAP_DIM
    other = jnp.where(lane < half, pltpu.roll(tile, LANES - half, 1), pltpu.roll(tile, half, 1))
    return tile * cosine + other * sine


def groups(cols):
    return max(g for g in (4, 2, 1) if cols % (g * LANES) == 0)


def kernel(
    n, tp, G, heads, prompt, fresh, wq, wk, wv, lam, gain,
    k_out, v_out, mix_out, gain_out,
    W, PR, acc, fr, XN, XM, wq_v, QS, QR, ct, st, qs, lam_v,
    w_recv, w_send, p_recv, p_send, x_recv, x_send, xt_recv, xt_send, q_recv, q_send, loc, token,
):
    _, rows, wl = prompt.shape
    depth, cols = wk.shape
    width = cols // G
    L = n // 4
    plane = 4 * depth
    me, mt = lax.axis_index("sp"), lax.axis_index("tp")
    z, y, x = me // 4, (me // 2) % 2, me % 2
    yf, xf = 1 - y, 1 - x
    up_ok, down_ok = z + 1 < L, z > 0
    outer = jnp.logical_not(up_ok & down_ok)

    first = [X if j < (G + 1) // 2 else Y for j in range(G)]
    second = [X + Y - f for f in first]
    wide = [G >= 4 and j % 2 == 1 for j in range(G)]
    order = [j for j in range(G) if not wide[j]] + [j for j in range(G) if wide[j]]
    wides = [j for j in range(G) if wide[j]]

    def at(zo, yo, xo):
        return zo * 4 + yo * 2 + xo

    def across(zo, axis):
        return at(zo, y, xf) if axis == X else at(zo, yf, x)

    partner = {X: at(z, y, xf), Y: at(z, yf, x), UP: me + 4, DOWN: me - 4}

    def piece(c, o):
        return W.at[c, pl.ds(pl.multiple_of(o * depth, depth), depth), :]

    def copy(c, d, o):
        return pltpu.make_async_remote_copy(
            src_ref=piece(c, o), dst_ref=piece(c, o),
            send_sem=w_send.at[d], recv_sem=w_recv.at[c * n + o],
            device_id={"sp": partner[d]}, device_id_type=pl.DeviceIdType.MESH,
        )

    def got(c, o):
        copy(c, X, o).wait_recv()

    def hop(c, o, dirs, wait=True):
        if wait:
            got(c, o)
        for d, ok in dirs:
            if ok is None:
                copy(c, d, o).start()
            else:
                pl.when(ok)(lambda d=d: copy(c, d, o).start())

    def own_sends(m):
        for j in range(G):
            hop(m * G + j, me, [(X, None), (UP, up_ok), (DOWN, down_ok)], wait=False)
        for j in sorted(range(G), key=lambda j: first[j] != Y):
            hop(m * G + j, me, [(Y, None)], wait=False)

    def in_plane(m, zo, along=()):
        for j in range(G):
            hop(m * G + j, across(zo, first[j]), list(along) + [(second[j], None)])

    def own_plane(m):
        in_plane(m, z, [(UP, outer & up_ok), (DOWN, outer & down_ok)])

    def own_wide(m):
        if not wides:
            return

        @pl.when(outer)
        def _():
            for other in (True, False):
                for j in wides:
                    o = across(z, second[j]) if other else at(z, yf, xf)
                    hop(m * G + j, o, [(UP, up_ok), (DOWN, down_ok)])

    def block(m, b, upper=True, lower=True):
        sides = [(z + 1 + b, L - 1 - z, down_ok, DOWN)] * upper + [(z - 1 - b, z, up_ok, UP)] * lower
        for zo, e, more, d in sides:
            if b < L - 2:
                @pl.when(b < e - 1)
                def _(zo=zo, more=more, d=d):
                    for j in order:
                        hop(m * G + j, at(zo, y, x), [(d, more), (first[j], None), (second[j], None)])
            end = 0 if d == UP else L - 1
            if b < L - 1:
                @pl.when(b == e - 1)
                def _(end=end, more=more, d=d):
                    for j in order:
                        far = [] if wide[j] else [(second[j], None)]
                        hop(m * G + j, at(end, y, x), [(d, more)] + far)
            if 1 <= b < L:
                @pl.when((b == e) & (e > 0))
                def _(end=end, more=more, d=d):
                    for j in order:
                        far = [] if wide[j] else [(second[j], None)]
                        hop(m * G + j, across(end, first[j]), [(d, more)] + far)
            if 2 <= b and wides:
                @pl.when((b == e + 1) & (e > 0))
                def _(end=end, more=more, d=d):
                    for other in (True, False):
                        for j in wides:
                            o = across(end, second[j]) if other else at(end, yf, xf)
                            hop(m * G + j, o, [(d, more)])

    def in_plane_of(m, s):
        if not 1 <= s <= L - 2:
            return
        for zo, ok in ((z + s, z + s < L - 1), (z - s, z - s > 0)):
            pl.when(ok)(lambda zo=zo: in_plane(m, zo))

    def loop(lo, hi, f):
        lax.fori_loop(lo, hi, lambda i, _: (f(i), _)[1], 0)

    R = min(rows, 512)

    near = jnp.minimum(z, L - 1 - z)
    far = jnp.where(z < L - 1 - z, 1, -1)

    def dots(m, t, last=False):
        turn = (t + 1) // 2 if t % 2 else -(t // 2)
        zo = z + far * jnp.where(t <= 2 * near, turn, t - near)
        thin = (zo > 0) & (zo < L - 1)
        for j in range(G):
            def rest_of(j=j):
                got(m * G + j, across(zo, second[j]))
                got(m * G + j, at(zo, yf, xf))
            if wide[j]:
                pl.when(thin)(rest_of)
            else:
                rest_of()

        def tile(i):
            r = pl.ds(pl.multiple_of(i * R, R), R)
            p = pl.ds(pl.multiple_of(zo * plane, plane), plane)
            for j in range(G):
                part = jnp.dot(PR[r, p], W[m * G + j, p, :], preferred_element_type=F32)
                if t > 0:
                    part = acc[j, r, :] + part
                if last:
                    v_out[r, pl.ds(j * width, width)] = part.astype(BF16)
                else:
                    acc[j, r, :] = part

        loop(0, rows // R, tile)

    barrier = pltpu.get_barrier_semaphore()
    for d in range(1, tp):
        pl.semaphore_signal(
            barrier, inc=1, device_id={"tp": (mt + d) % tp}, device_id_type=pl.DeviceIdType.MESH)

    def signal(sem, d):
        pl.semaphore_signal(
            sem, inc=1, device_id={"sp": partner[d]}, device_id_type=pl.DeviceIdType.MESH)

    signal(barrier, X)
    signal(barrier, Y)
    pl.when(up_ok)(lambda: signal(barrier, UP))
    pl.when(down_ok)(lambda: signal(barrier, DOWN))

    def columns(t):
        return PR.at[:, pl.ds(pl.multiple_of(t * wl, wl), wl)]

    own = [
        pltpu.make_async_copy(
            w.at[:, pl.ds(j * width, width)], piece(m * G + j, me), loc.at[m])
        for m, w in enumerate((wk, wv)) for j in range(G)
    ]
    rest = [
        pltpu.make_async_copy(src, dst, loc.at[2 + i])
        for i, (src, dst) in enumerate((
            (fresh, fr), (prompt.at[0], columns(mt)), (wq, wq_v), (lam, lam_v), (gain, gain_out)))
    ]

    def own_wait(m):
        whole = W.at[pl.ds(m * G, G), pl.ds(pl.multiple_of(me * depth, depth), depth), :]
        pltpu.make_async_copy(whole, whole, loc.at[m]).wait()

    for c in own[:G]:
        c.start()
    rest[0].start()
    for c in own[G:]:
        c.start()
    for c in rest[1:]:
        c.start()
    own_wait(0)

    @pl.when(up_ok & down_ok)
    def _():
        pl.semaphore_wait(barrier, 4 + tp - 1)

    @pl.when(outer)
    def _():
        pl.semaphore_wait(barrier, 3 + tp - 1)

    own_sends(0)

    def x_copy(d):
        return pltpu.make_async_remote_copy(
            src_ref=XN.at[mt, me], dst_ref=XN.at[mt, me],
            send_sem=x_send.at[0], recv_sem=x_recv.at[0],
            device_id={"sp": (me + d) % n}, device_id_type=pl.DeviceIdType.MESH,
        )

    def together(ref, send_sem, recv_sem):
        return pltpu.make_async_remote_copy(
            src_ref=ref, dst_ref=ref, send_sem=send_sem.at[0], recv_sem=recv_sem.at[0],
            device_id={"sp": partner[X]}, device_id_type=pl.DeviceIdType.MESH,
        )

    x_all = together(XN.at[0, pl.ds(0, n - 1)], x_send, x_recv)
    q_all = together(QR.at[pl.ds(0, n - 1)], q_send, q_recv)

    def p_copy(d):
        return pltpu.make_async_remote_copy(
            src_ref=prompt.at[0], dst_ref=columns(mt),
            send_sem=p_send.at[d], recv_sem=p_recv.at[mt],
            device_id={"tp": (mt + d) % tp}, device_id_type=pl.DeviceIdType.MESH,
        )

    def p_wait(d):
        src = (mt + d) % tp
        return pltpu.make_async_remote_copy(
            src_ref=columns(src), dst_ref=columns(src),
            send_sem=p_send.at[d], recv_sem=p_recv.at[src],
            device_id={"tp": src}, device_id_type=pl.DeviceIdType.MESH,
        )

    signal(token.at[Y], Y)

    def relay_token(b):
        for turn, before, more, d in ((z == b, down_ok, up_ok, UP), (z == L - 1 - b, up_ok, down_ok, DOWN)):
            pl.when(turn & before)(lambda d=d: pl.semaphore_wait(token.at[d], 1))
            pl.when(turn & more)(lambda d=d: signal(token.at[d], d))

    rest[0].wait()
    XN[mt, me] = fr[...].astype(F32)
    own_wait(1)
    for d in range(1, tp):
        p_copy(d).start()


    def xt_copy(d, t):
        return pltpu.make_async_remote_copy(
            src_ref=XN.at[t], dst_ref=XN.at[t],
            send_sem=xt_send.at[d], recv_sem=xt_recv.at[t],
            device_id={"tp": (mt + d) % tp}, device_id_type=pl.DeviceIdType.MESH,
        )

    def q_copy(d):
        dst = (me + d) % n
        return pltpu.make_async_remote_copy(
            src_ref=QS.at[dst], dst_ref=QR.at[me],
            send_sem=q_send.at[0], recv_sem=q_recv.at[0],
            device_id={"sp": dst}, device_id_type=pl.DeviceIdType.MESH,
        )

    def share_new():
        x_all.wait_recv()
        for d in range(1, tp):
            xt_copy(d, mt).start()

    def partial_queries():
        for d in range(1, tp):
            xt_copy(d, (mt + d) % tp).wait_recv()
        begin = me * depth
        holder, offset = begin // wl, begin % wl
        for j in range(n):
            XM[pl.ds(j, 1), :] = XN[holder, j]
        pick = (
            lax.broadcasted_iota(jnp.int32, (wl, depth), 0)
            == offset + lax.broadcasted_iota(jnp.int32, (wl, depth), 1)
        )
        chosen = jnp.dot(
            XM[...].astype(BF16), jnp.where(pick, 1.0, 0.0).astype(BF16), preferred_element_type=F32
        ).astype(BF16)
        rest[2].wait()
        partial = jnp.dot(chosen, wq_v[...], preferred_element_type=F32)
        for j in range(n):
            QS[j] = partial[j:j + 1, :]
        QR[me] = QS[me]
        loop(1, n, lambda d: q_copy(d).start())

    hp = max(heads, 8)
    pad = 2 * hp

    def build_query():
        qcos, qsin = table(jnp.full((8, LANES), rows, F32))
        q_all.wait_recv()
        total = QR[0]
        for j in range(1, n):
            total = total + QR[j]
        total = jnp.broadcast_to(total, (8, cols))
        query = jnp.concatenate(
            [rotated(total[:, i:i + LANES], qcos, qsin) for i in range(0, cols, LANES)], axis=1)
        query = jnp.broadcast_to(query[:1], (pad, cols))
        row = lax.broadcasted_iota(jnp.int32, (pad, cols), 0)
        keep = 2 * (row % hp) + row // hp == lax.broadcasted_iota(jnp.int32, (pad, cols), 1) // MAP_DIM
        qs[...] = jnp.where(keep, query, 0.0).astype(BF16)

    def angles(i):
        position = (i * 64 + lax.broadcasted_iota(jnp.int32, (64, LANES), 0)).astype(F32)
        r = pl.ds(pl.multiple_of(i * 64, 64), 64)
        ct[r, :], st[r, :] = table(position)

    RR = min(rows, 256)

    def rotate_rows(i):
        r = pl.ds(pl.multiple_of(i * RR, RR), RR)
        cosine, sine = ct[r, :], st[r, :]
        for i in range(0, cols, LANES):
            tile = acc[i // width, r, pl.ds(i % width, LANES)]
            k_out[r, pl.ds(i, LANES)] = rotated(tile, cosine, sine).astype(BF16)

    def weigh():
        scores = lax.dot_general(
            qs[...], k_out[...], (((1,), (1,)), ((), ())), preferred_element_type=F32) * MAP_DIM ** -0.5
        weights = jnp.exp(scores - jnp.max(scores, axis=-1, keepdims=True))
        weights = weights / jnp.sum(weights, axis=-1, keepdims=True)
        rest[3].wait()
        here = (lax.broadcasted_iota(jnp.int32, (hp, heads), 0)
                == lax.broadcasted_iota(jnp.int32, (hp, heads), 1))
        scale = jnp.sum(jnp.where(here, lam_v[...], 0.0), axis=-1, keepdims=True)
        mix = weights[:hp] - scale * weights[hp:]
        high = mix.astype(BF16)
        left = mix - high.astype(F32)
        mid = left.astype(BF16)
        low = (left - mid.astype(F32)).astype(BF16)
        mix_out[...] = jnp.concatenate([high, mid, low], axis=0)

    own_plane(0)
    pl.semaphore_wait(token.at[Y], 1)
    signal(token.at[X], X)
    steps = iter(range(L))

    def pass_token():
        for b in steps:
            relay_token(b)
            break

    block(0, 0, upper=True, lower=False)
    pl.semaphore_wait(token.at[X], 1)
    pass_token()
    block(0, 0, upper=False)
    pass_token()
    own_wide(0)
    pass_token()
    for b in range(1, L + 1):
        block(0, b, lower=False)
        pass_token()
        block(0, b, upper=False)
        if b == 1:
            own_sends(1)
        in_plane_of(0, b)
        if b == max(1, L - 3):
            for k in steps:
                relay_token(k)
            loop(1, n, lambda d: x_copy(d).start())
        if b == 1:
            own_plane(1)
            rest[1].wait()
            for d in range(1, tp):
                p_wait(d).wait_recv()
            dots(0, 0)
        if b == min(2, L):
            own_wide(1)
        if b == min(3, L):
            loop(0, rows // 64, angles)
            share_new()
        if b >= 3:
            dots(0, b - 2)

    partial_queries()
    for b in range(L + 1):
        if b == L > 2:
            dots(1, L - 2)
        block(1, b)
        in_plane_of(1, b)
        if b == 0:
            if L > 1:
                dots(0, L - 1)
            loop(0, rows // RR, rotate_rows)
        if b == 1 and L > 1:
            dots(1, 0)
        if b == min(2, L):
            build_query()
            weigh()
        if 3 <= b < L:
            dots(1, b - 2)
    dots(1, L - 1, last=True)
    rest[4].wait()
    x_all.wait_send()
    q_all.wait_send()
    for d in range(1, tp):
        p_copy(d).wait_send()
        xt_copy(d, mt).wait_send()

    def sent(d, pieces):
        all_of = W.at[:, pl.ds(0, pieces * depth // G), :]
        pltpu.make_async_remote_copy(
            src_ref=all_of, dst_ref=all_of, send_sem=w_send.at[d], recv_sem=w_recv.at[0],
            device_id={"sp": partner[X]}, device_id_type=pl.DeviceIdType.MESH,
        ).wait_send()

    def plane_pieces(d, inner, outers):
        turned = sum(s == d for s in second)
        halves = 2 * sum(s == d and not w for s, w in zip(second, wide))
        return (inner + 1) * (G + turned) + outers * halves

    def settle(inner, outers):
        for d in (X, Y):
            sent(d, plane_pieces(d, inner, outers))

    pl.when(outer)(lambda: settle(max(L - 2, 0), min(L - 1, 1)))
    if L > 2:
        pl.when(jnp.logical_not(outer))(lambda: settle(L - 3, 2))
    total = 0
    for k in range(L - 1):
        total += G if 0 < k else 2 * G + 2 * len(wides)
        pl.when(z == k)(lambda total=total: sent(UP, total))
        pl.when(z == L - 1 - k)(lambda total=total: sent(DOWN, total))


def read(keys, values, mix, gain, k_out, v_out, read_out, sem):
    hp = mix.shape[0] // 3
    heads = read_out.shape[1]
    k_copy = pltpu.make_async_copy(keys, k_out.at[0], sem.at[0])
    v_copy = pltpu.make_async_copy(values, v_out.at[0], sem.at[1])
    v_copy.start()
    k_copy.start()
    mixed = jnp.dot(mix[...], values[...], preferred_element_type=F32)
    mixed = mixed[:hp] + mixed[hp:2 * hp] + mixed[2 * hp:]
    diff = jnp.concatenate(
        [mixed[h:h + 1, h * VAL_DIM:(h + 1) * VAL_DIM] for h in range(heads)], axis=0)
    normed = diff * lax.rsqrt(jnp.mean(diff * diff, axis=-1, keepdims=True) + norm_eps)
    read_out[0] = (normed * gain[...]).astype(BF16)
    v_copy.wait()
    k_copy.wait()


def body(n, tp, prompt, new_input, w_query, w_key, w_value, lam, out_gain):
    seqs, rows, wl = prompt.shape
    depth, cols = w_key.shape
    heads = lam.shape[0]
    G = groups(cols)
    hp = max(heads, 8)
    operands = [
        pltpu.with_memory_space_constraint(a, pltpu.HBM)
        for a in (prompt, new_input, w_query, w_key, w_value, lam[None, :], out_gain[None, :])
    ]
    any_ = pl.BlockSpec(memory_space=pl.ANY)
    hbm = pl.BlockSpec(memory_space=pltpu.HBM)
    vmem = pl.BlockSpec(memory_space=pltpu.VMEM)
    dma = pltpu.SemaphoreType.DMA
    keys, values, mix, gain = pl.pallas_call(
        functools.partial(kernel, n, tp, G, heads),
        out_shape=(
            pltpu.VMEM((rows, cols), BF16),
            pltpu.VMEM((rows, cols), BF16),
            pltpu.VMEM((3 * hp, rows), BF16),
            pltpu.VMEM((1, VAL_DIM), F32),
        ),
        in_specs=[hbm] * 7,
        out_specs=(vmem, vmem, vmem, vmem),
        scratch_shapes=[
            pltpu.VMEM((2 * G, n * depth, cols // G), BF16),
            pltpu.VMEM((rows, tp * wl), BF16),
            pltpu.VMEM((G, rows, cols // G), F32),
            pltpu.VMEM((1, wl), BF16),
            pltpu.VMEM((tp, n, 1, wl), F32),
            pltpu.VMEM((n, wl), F32),
            pltpu.VMEM((depth, cols), BF16),
            pltpu.VMEM((n, 1, cols), F32),
            pltpu.VMEM((n, 1, cols), F32),
            pltpu.VMEM((rows, LANES), F32),
            pltpu.VMEM((rows, LANES), F32),
            pltpu.VMEM((2 * hp, cols), BF16),
            pltpu.VMEM((1, heads), F32),
            dma((2 * G * n,)), dma((4,)), dma((tp,)), dma((tp,)), dma((1,)), dma((1,)),
            dma((tp,)), dma((tp,)), dma((1,)), dma((1,)), dma((7,)),
            pltpu.SemaphoreType.REGULAR((4,)),
        ],
        compiler_params=pltpu.CompilerParams(
            collective_id=0, has_side_effects=True, vmem_limit_bytes=44 * 1024 * 1024),
        name="prefill",
    )(*operands)
    return pl.pallas_call(
        read,
        out_shape=(
            jax.ShapeDtypeStruct((seqs, rows, cols), BF16),
            jax.ShapeDtypeStruct((seqs, rows, cols), BF16),
            jax.ShapeDtypeStruct((seqs, heads, VAL_DIM), BF16),
        ),
        in_specs=[vmem] * 4,
        out_specs=(any_, any_, vmem),
        scratch_shapes=[dma((2,))],
        compiler_params=pltpu.CompilerParams(vmem_limit_bytes=24 * 1024 * 1024),
        name="read",
    )(keys, values, mix, gain)


def solution(mesh):
    in_specs = (
        P("sp", None, "tp"), P("sp", "tp"), P("sp", "tp"), P("sp", "tp"), P("sp", "tp"), P("tp"), P(),
    )
    out_specs = (P("sp", None, "tp"), P("sp", None, "tp"), P("sp", "tp", None))
    return jax.shard_map(
        functools.partial(body, mesh.shape["sp"], mesh.shape["tp"]),
        mesh=mesh, in_specs=in_specs, out_specs=out_specs, check_vma=False)
```

time: 90.4 us -> 71.6 us (0.79)
  Pallas kernels: 88.9 us -> 70.8 us
    pallas_call x1, Pallas kernels: 83.7 us -> 68.2 us  [body(): pl.pallas_call(functools.partial(kernel, n, tp, G, heads), out_shape=(plt...]
    pallas_call x1, Pallas kernels: 5.17 us -> 2.64 us  [body(): pl.pallas_call(read, out_shape=(jax.ShapeDtypeStruct((seqs, rows, cols),...]
where the time goes in v1:
time: 71.6 us; the launch traced here: 71.5 us
  Pallas kernels  70.8 us (99%)
    pallas_call x1, Pallas kernels, body(): pl.pallas_call(functools.partial(kernel, n, tp, G, heads), out_shape=(plt...  68.2 us
    pallas_call x1, Pallas kernels, body(): pl.pallas_call(read, out_shape=(jax.ShapeDtypeStruct((seqs, rows, cols),...  2.64 us

profile of v1, /device:TPU:0, one launch (start us, length us, event | category | flops | bytes accessed | tf_op | source)
XLA Modules:
  0.0 71.5 jit_solution(6154398378709157238)
XLA Ops:
  0.6 68.2 %prefill.1 = (bf16[1024,1024]{1,0:T(8,128)(2,1)S(1)}, bf16[1024,1024]{1,0:T(8,128)(2,1)S(1)}, bf16[24,1024]{1,0:T(8,128)(2,1)S(1)}, f32[1,128]{1,0:T(1,128)S(1)}) custom-call(bf16[1,1024,1024]{2,1,0:T(8,128)(2,1)} %prompt.1, bf16[1,1024]{1,0:T(2,128)(2,1)} %fresh.1, bf16[128,1024]{1,0:T(8,128)(2,1)} %wq.1, bf16[128,1024]{1,0:T(8,128)(2,1)} %wk.1, ...), custom_call_target="tpu_custom_call" | custom-call | tf_op jit(solution)/shard_map/prefill/pallas_call | solution.py:499
  68.8 2.6 %read.1 = (bf16[1,1024,1024]{2,1,0:T(8,128)(2,1)}, bf16[1,1024,1024]{2,1,0:T(8,128)(2,1)}, bf16[1,8,128]{2,1,0:T(8,128)(2,1)}) custom-call(bf16[1024,1024]{1,0:T(8,128)(2,1)S(1)} %get-tuple-element.7.keys, bf16[1024,1024]{1,0:T(8,128)(2,1)S(1)} %get-tuple-element.8.values, bf16[24,1024]{1,0:T(8,128)(2,1)S(1)} %get-tuple-element.9.mix, ...), custom_call_target="tpu_custom_call" | custom-call | tf_op jit(solution)/shard_map/read/pallas_call | solution.py:531

commit v2 on v1

--- a/solution.py
+++ b/solution.py
@@ -1,4 +1,5 @@
 import functools
+import heapq
 import math
 
 import jax
@@ -15,6 +16,8 @@
 norm_eps = 1e-05
 
 X, Y, UP, DOWN = 0, 1, 2, 3
+LAG, LEAD = 0.9, 3.0
+TOK0, TOK1 = 2.5, 4.0
 F32, BF16 = jnp.float32, jnp.bfloat16
 
 
@@ -41,11 +44,99 @@
     return max(g for g in (4, 2, 1) if cols % (g * LANES) == 0)
 
 
+class Plan:
+    def __init__(self, L, G):
+        self.L, self.G = L, G
+        self.first = [X if j < (G + 1) // 2 else Y for j in range(G)]
+        self.wide = [G >= 4 and j % 2 == 1 for j in range(G)]
+        self.arrival = [{} for _ in range(L)]
+        self.start = [{} for _ in range(L)]
+        waiting = {(z, d): [] for z in range(L) for d in range(4)}
+        free = dict.fromkeys(waiting, 0.0)
+        events, count = [], 0
+
+        def post(time, what):
+            nonlocal count
+            count += 1
+            heapq.heappush(events, (time, count, what))
+
+        def begin(z, d, time):
+            if waiting[z, d] and free[z, d] <= time:
+                piece = heapq.heappop(waiting[z, d])[-1]
+                self.start[z][piece, d] = time
+                free[z, d] = time + 1
+                post(time + 1, (z, d, None))
+                post(time + 1 + LAG, (*self.beyond(z, piece, d)[:1], None, self.beyond(z, piece, d)[1]))
+
+        for z in range(L):
+            for m in range(2):
+                for j in range(G):
+                    post(0.0, (z, None, (m, j, z, 0, 0)))
+        while events:
+            time, _, (z, d, piece) = heapq.heappop(events)
+            if d is not None:
+                begin(z, d, time)
+                continue
+            assert piece not in self.arrival[z]
+            self.arrival[z][piece] = time
+            for d in self.links(z, piece):
+                count += 1
+                goes_on = bool(self.links(*self.beyond(z, piece, d)))
+                heapq.heappush(waiting[z, d], (self.rank(z, piece, d), count, piece))
+            for d in range(4):
+                begin(z, d, time)
+        self.end = max(max(a.values()) for a in self.arrival)
+
+    def rank(self, z, piece, d):
+        m, j, zo, dy, dx = piece
+        there, seen = self.beyond(z, piece, d)
+        relayed = any(link in (X, Y) for link in self.links(there, seen))
+        return m, not relayed
+
+    def outer(self, zo):
+        return zo in (0, self.L - 1)
+
+    def links(self, z, piece):
+        m, j, zo, dy, dx = piece
+        along = [d for d, step in ((UP, 1), (DOWN, -1))
+                 if 0 <= z + step < self.L and (z == zo or (step > 0) == (z > zo))]
+        second = [X + Y - self.first[j]]
+        if (dy, dx) == (0, 0):
+            if z == zo or not self.outer(zo):
+                return along + [X, Y]
+            return along + second * (not self.wide[j])
+        if (dx if self.first[j] == X else dy) and not (dx and dy):
+            along = along * self.outer(zo)
+            return along + second * (z == zo or not self.outer(zo) or not self.wide[j])
+        return along * (self.outer(zo) and self.wide[j])
+
+    def beyond(self, z, piece, d):
+        m, j, zo, dy, dx = piece
+        return z + (d == UP) - (d == DOWN), (m, j, zo, dy ^ (d == Y), dx ^ (d == X))
+
+    def roles(self):
+        return range((self.L + 1) // 2)
+
+    def sends(self, k):
+        own = ((max(self.arrival[k][p], t - LEAD), t, p, d) for (p, d), t in self.start[k].items())
+        return [(when, p, d) for when, _, p, d in sorted(own)]
+
+    def pieces(self, m, zo, groups):
+        return [(m, j, zo, dy, dx) for j in groups for dy in range(2) for dx in range(2)]
+
+    def ready(self, k, m, zo, groups):
+        return max(self.arrival[k][p] for p in self.pieces(m, zo, groups))
+
+    def order(self, k, m):
+        everything = range(self.G)
+        return sorted(range(self.L), key=lambda zo: (zo != k, self.ready(k, m, zo, everything)))
+
+
 def kernel(
     n, tp, G, heads, prompt, fresh, wq, wk, wv, lam, gain,
     k_out, v_out, mix_out, gain_out,
-    W, PR, acc, fr, XN, XM, wq_v, QS, QR, ct, st, qs, lam_v,
-    w_recv, w_send, p_recv, p_send, x_recv, x_send, xt_recv, xt_send, q_recv, q_send, loc, token,
+    W, PR, acc, fr, XR, XM, wq_v, QS, QR, ct, st, qs, lam_v,
+    w_recv, w_send, p_recv, p_send, x_recv, x_send, q_recv, q_send, loc, token,
 ):
     _, rows, wl = prompt.shape
     depth, cols = wk.shape
@@ -58,126 +149,72 @@
     up_ok, down_ok = z + 1 < L, z > 0
     outer = jnp.logical_not(up_ok & down_ok)
 
-    first = [X if j < (G + 1) // 2 else Y for j in range(G)]
-    second = [X + Y - f for f in first]
-    wide = [G >= 4 and j % 2 == 1 for j in range(G)]
-    order = [j for j in range(G) if not wide[j]] + [j for j in range(G) if wide[j]]
-    wides = [j for j in range(G) if wide[j]]
+    plan = Plan(L, G)
+    role = jnp.minimum(z, L - 1 - z)
+    ahead = jnp.where(z <= L - 1 - z, 1, -1)
 
     def at(zo, yo, xo):
         return zo * 4 + yo * 2 + xo
 
-    def across(zo, axis):
-        return at(zo, y, xf) if axis == X else at(zo, yf, x)
-
     partner = {X: at(z, y, xf), Y: at(z, yf, x), UP: me + 4, DOWN: me - 4}
 
     def piece(c, o):
         return W.at[c, pl.ds(pl.multiple_of(o * depth, depth), depth), :]
+
+    target = {X: partner[X], Y: partner[Y], UP: me + 4 * ahead, DOWN: me - 4 * ahead}
+
+    def place(k, p):
+        m, j, zo, dy, dx = p
+        return m * G + j, at(z + ahead * (zo - k), yf if dy else y, xf if dx else x)
 
     def copy(c, d, o):
         return pltpu.make_async_remote_copy(
             src_ref=piece(c, o), dst_ref=piece(c, o),
             send_sem=w_send.at[d], recv_sem=w_recv.at[c * n + o],
-            device_id={"sp": partner[d]}, device_id_type=pl.DeviceIdType.MESH,
+            device_id={"sp": target[d]}, device_id_type=pl.DeviceIdType.MESH,
         )
 
-    def got(c, o):
-        copy(c, X, o).wait_recv()
-
-    def hop(c, o, dirs, wait=True):
-        if wait:
-            got(c, o)
-        for d, ok in dirs:
-            if ok is None:
+    def by_role(f):
+        for k in plan.roles():
+            pl.when(role == k)(functools.partial(f, k))
+
+    pending = {k: plan.sends(k) for k in plan.roles()}
+    arrived = {k: set(plan.pieces(0, k, range(0))) for k in plan.roles()}
+
+    def need(k, p):
+        if p[2:] != (k, 0, 0) and p not in arrived[k]:
+            arrived[k].add(p)
+            c, o = place(k, p)
+            copy(c, X, o).wait_recv()
+
+    def advance(time, wanted=lambda k: ()):
+        def go(k):
+            while pending[k] and pending[k][0][0] < time:
+                _, p, d = pending[k].pop(0)
+                need(k, p)
+                c, o = place(k, p)
                 copy(c, d, o).start()
-            else:
-                pl.when(ok)(lambda d=d: copy(c, d, o).start())
-
-    def own_sends(m):
-        for j in range(G):
-            hop(m * G + j, me, [(X, None), (UP, up_ok), (DOWN, down_ok)], wait=False)
-        for j in sorted(range(G), key=lambda j: first[j] != Y):
-            hop(m * G + j, me, [(Y, None)], wait=False)
-
-    def in_plane(m, zo, along=()):
-        for j in range(G):
-            hop(m * G + j, across(zo, first[j]), list(along) + [(second[j], None)])
-
-    def own_plane(m):
-        in_plane(m, z, [(UP, outer & up_ok), (DOWN, outer & down_ok)])
-
-    def own_wide(m):
-        if not wides:
-            return
-
-        @pl.when(outer)
-        def _():
-            for other in (True, False):
-                for j in wides:
-                    o = across(z, second[j]) if other else at(z, yf, xf)
-                    hop(m * G + j, o, [(UP, up_ok), (DOWN, down_ok)])
-
-    def block(m, b, upper=True, lower=True):
-        sides = [(z + 1 + b, L - 1 - z, down_ok, DOWN)] * upper + [(z - 1 - b, z, up_ok, UP)] * lower
-        for zo, e, more, d in sides:
-            if b < L - 2:
-                @pl.when(b < e - 1)
-                def _(zo=zo, more=more, d=d):
-                    for j in order:
-                        hop(m * G + j, at(zo, y, x), [(d, more), (first[j], None), (second[j], None)])
-            end = 0 if d == UP else L - 1
-            if b < L - 1:
-                @pl.when(b == e - 1)
-                def _(end=end, more=more, d=d):
-                    for j in order:
-                        far = [] if wide[j] else [(second[j], None)]
-                        hop(m * G + j, at(end, y, x), [(d, more)] + far)
-            if 1 <= b < L:
-                @pl.when((b == e) & (e > 0))
-                def _(end=end, more=more, d=d):
-                    for j in order:
-                        far = [] if wide[j] else [(second[j], None)]
-                        hop(m * G + j, across(end, first[j]), [(d, more)] + far)
-            if 2 <= b and wides:
-                @pl.when((b == e + 1) & (e > 0))
-                def _(end=end, more=more, d=d):
-                    for other in (True, False):
-                        for j in wides:
-                            o = across(end, second[j]) if other else at(end, yf, xf)
-                            hop(m * G + j, o, [(d, more)])
-
-    def in_plane_of(m, s):
-        if not 1 <= s <= L - 2:
-            return
-        for zo, ok in ((z + s, z + s < L - 1), (z - s, z - s > 0)):
-            pl.when(ok)(lambda zo=zo: in_plane(m, zo))
+            for p in wanted(k):
+                need(k, p)
+
+        by_role(go)
 
     def loop(lo, hi, f):
         lax.fori_loop(lo, hi, lambda i, _: (f(i), _)[1], 0)
 
     R = min(rows, 512)
 
-    near = jnp.minimum(z, L - 1 - z)
-    far = jnp.where(z < L - 1 - z, 1, -1)
-
-    def dots(m, t, last=False):
-        turn = (t + 1) // 2 if t % 2 else -(t // 2)
-        zo = z + far * jnp.where(t <= 2 * near, turn, t - near)
-        thin = (zo > 0) & (zo < L - 1)
-        for j in range(G):
-            def rest_of(j=j):
-                got(m * G + j, across(zo, second[j]))
-                got(m * G + j, at(zo, yf, xf))
-            if wide[j]:
-                pl.when(thin)(rest_of)
-            else:
-                rest_of()
+    turns = {(k, m): plan.order(k, m) for k in plan.roles() for m in range(2)}
+
+    def dots(m, t, groups=range(G), last=False):
+        zo = z
+        for k in plan.roles():
+            zo = jnp.where(role == k, z + ahead * (turns[k, m][t] - k), zo)
 
         def tile(i):
             r = pl.ds(pl.multiple_of(i * R, R), R)
             p = pl.ds(pl.multiple_of(zo * plane, plane), plane)
-            for j in range(G):
+            for j in groups:
                 part = jnp.dot(PR[r, p], W[m * G + j, p, :], preferred_element_type=F32)
                 if t > 0:
                     part = acc[j, r, :] + part
@@ -237,14 +274,32 @@
     def _():
         pl.semaphore_wait(barrier, 3 + tp - 1)
 
-    own_sends(0)
-
-    def x_copy(d):
-        return pltpu.make_async_remote_copy(
-            src_ref=XN.at[mt, me], dst_ref=XN.at[mt, me],
-            send_sem=x_send.at[0], recv_sem=x_recv.at[0],
-            device_id={"sp": (me + d) % n}, device_id_type=pl.DeviceIdType.MESH,
-        )
+
+    block_of = XR.shape[2]
+    share = wl // depth
+    mine = me // share == mt
+
+    def features(chip):
+        first_one = (chip * depth) % wl // block_of * block_of
+        return pl.ds(pl.multiple_of(first_one, block_of), block_of)
+
+    def x_sends():
+        def to(i):
+            chip, t = mt * share + (me + i // tp) % share, (mt + i) % tp
+
+            @pl.when((chip != me) | (t != mt))
+            def _():
+                pltpu.make_async_remote_copy(
+                    src_ref=fr.at[:, features(chip)], dst_ref=XR.at[me],
+                    send_sem=x_send.at[0], recv_sem=x_recv.at[0],
+                    device_id={"sp": chip, "tp": t}, device_id_type=pl.DeviceIdType.MESH,
+                ).start()
+
+        loop(0, n, to)
+
+        @pl.when(mine)
+        def _():
+            XR[me] = fr[:, features(me)]
 
     def together(ref, send_sem, recv_sem):
         return pltpu.make_async_remote_copy(
@@ -252,7 +307,10 @@
             device_id={"sp": partner[X]}, device_id_type=pl.DeviceIdType.MESH,
         )
 
-    x_all = together(XN.at[0, pl.ds(0, n - 1)], x_send, x_recv)
+    def x_wait(end):
+        pl.when(mine)(lambda: end(together(XR.at[pl.ds(0, n - 1)], x_send, x_recv)))
+        pl.when(jnp.logical_not(mine))(lambda: end(together(XR, x_send, x_recv)))
+
     q_all = together(QR.at[pl.ds(0, n - 1)], q_send, q_recv)
 
     def p_copy(d):
@@ -270,6 +328,7 @@
             device_id={"tp": src}, device_id_type=pl.DeviceIdType.MESH,
         )
 
+    advance(0.0001)
     signal(token.at[Y], Y)
 
     def relay_token(b):
@@ -278,18 +337,10 @@
             pl.when(turn & more)(lambda d=d: signal(token.at[d], d))
 
     rest[0].wait()
-    XN[mt, me] = fr[...].astype(F32)
     own_wait(1)
     for d in range(1, tp):
         p_copy(d).start()
 
-
-    def xt_copy(d, t):
-        return pltpu.make_async_remote_copy(
-            src_ref=XN.at[t], dst_ref=XN.at[t],
-            send_sem=xt_send.at[d], recv_sem=xt_recv.at[t],
-            device_id={"tp": (mt + d) % tp}, device_id_type=pl.DeviceIdType.MESH,
-        )
 
     def q_copy(d):
         dst = (me + d) % n
@@ -299,25 +350,18 @@
             device_id={"sp": dst}, device_id_type=pl.DeviceIdType.MESH,
         )
 
-    def share_new():
-        x_all.wait_recv()
-        for d in range(1, tp):
-            xt_copy(d, mt).start()
-
     def partial_queries():
-        for d in range(1, tp):
-            xt_copy(d, (mt + d) % tp).wait_recv()
-        begin = me * depth
-        holder, offset = begin // wl, begin % wl
+        x_wait(lambda c: c.wait_recv())
         for j in range(n):
-            XM[pl.ds(j, 1), :] = XN[holder, j]
-        pick = (
-            lax.broadcasted_iota(jnp.int32, (wl, depth), 0)
-            == offset + lax.broadcasted_iota(jnp.int32, (wl, depth), 1)
-        )
-        chosen = jnp.dot(
-            XM[...].astype(BF16), jnp.where(pick, 1.0, 0.0).astype(BF16), preferred_element_type=F32
-        ).astype(BF16)
+            XM[pl.ds(j, 1), :] = XR[j].astype(F32)
+        chosen = XM[...].astype(BF16)
+        if block_of > depth:
+            pick = (
+                lax.broadcasted_iota(jnp.int32, (block_of, depth), 0)
+                == me * depth % block_of + lax.broadcasted_iota(jnp.int32, (block_of, depth), 1)
+            )
+            chosen = jnp.dot(
+                chosen, jnp.where(pick, 1.0, 0.0).astype(BF16), preferred_element_type=F32).astype(BF16)
         rest[2].wait()
         partial = jnp.dot(chosen, wq_v[...], preferred_element_type=F32)
         for j in range(n):
@@ -372,72 +416,62 @@
         low = (left - mid.astype(F32)).astype(BF16)
         mix_out[...] = jnp.concatenate([high, mid, low], axis=0)
 
-    own_plane(0)
-    pl.semaphore_wait(token.at[Y], 1)
-    signal(token.at[X], X)
-    steps = iter(range(L))
-
-    def pass_token():
-        for b in steps:
-            relay_token(b)
-            break
-
-    block(0, 0, upper=True, lower=False)
-    pl.semaphore_wait(token.at[X], 1)
-    pass_token()
-    block(0, 0, upper=False)
-    pass_token()
-    own_wide(0)
-    pass_token()
-    for b in range(1, L + 1):
-        block(0, b, lower=False)
-        pass_token()
-        block(0, b, upper=False)
-        if b == 1:
-            own_sends(1)
-        in_plane_of(0, b)
-        if b == max(1, L - 3):
-            for k in steps:
-                relay_token(k)
-            loop(1, n, lambda d: x_copy(d).start())
-        if b == 1:
-            own_plane(1)
-            rest[1].wait()
-            for d in range(1, tp):
-                p_wait(d).wait_recv()
-            dots(0, 0)
-        if b == min(2, L):
-            own_wide(1)
-        if b == min(3, L):
-            loop(0, rows // 64, angles)
-            share_new()
-        if b >= 3:
-            dots(0, b - 2)
-
-    partial_queries()
-    for b in range(L + 1):
-        if b == L > 2:
-            dots(1, L - 2)
-        block(1, b)
-        in_plane_of(1, b)
-        if b == 0:
-            if L > 1:
-                dots(0, L - 1)
-            loop(0, rows // RR, rotate_rows)
-        if b == 1 and L > 1:
-            dots(1, 0)
-        if b == min(2, L):
-            build_query()
-            weigh()
-        if 3 <= b < L:
-            dots(1, b - 2)
-    dots(1, L - 1, last=True)
+    def when_ready(m, t, groups):
+        return max(plan.ready(k, m, turns[k, m][t], groups) for k in plan.roles())
+
+    def prompt_whole():
+        rest[1].wait()
+        for d in range(1, tp):
+            p_wait(d).wait_recv()
+
+    def first_token():
+        pl.semaphore_wait(token.at[Y], 1)
+        signal(token.at[X], X)
+
+    def second_token():
+        pl.semaphore_wait(token.at[X], 1)
+        relay_token(0)
+
+    def turn_rows(i):
+        loop(i * (rows // RR) // 2, (i + 1) * (rows // RR) // 2, rotate_rows)
+
+    none = lambda k: ()
+    work = [
+        (TOK0, first_token, none), (TOK1, second_token, none),
+        *((TOK1 + 0.9 * b, functools.partial(relay_token, b), none) for b in range(1, L)),
+    ]
+    sent_x = TOK1 + 0.9 * L
+    work.append((sent_x, x_sends, none))
+    work.append((sent_x + 9, partial_queries, none))
+    work.append((sent_x + 4, lambda: loop(0, rows // 64, angles), none))
+    keys_at = 0
+    for m in range(2):
+        for t in range(L):
+            last = m == 1 and t == L - 1
+            when = when_ready(m, t, range(G)) + 0.1
+            if m == 0 and t == 0:
+                work.append((when, prompt_whole, none))
+            if m == 1 and t == 0:
+                when = max(when, keys_at + 2.5)
+            if m == 0:
+                keys_at = max(keys_at, when)
+            work.append((
+                when + 0.001 * t, functools.partial(dots, m, t, last=last),
+                lambda k, m=m, t=t: plan.pieces(m, turns[k, m][t], range(G))))
+    work.append((keys_at + 0.1, lambda: turn_rows(0), none))
+    work.append((keys_at + 1.3, lambda: turn_rows(1), none))
+    answer = max(sent_x + 9 + 12, keys_at + 2.4)
+    work.append((answer, build_query, none))
+    work.append((answer + 0.5, weigh, none))
+    for time, act, wanted in sorted(work, key=lambda item: item[0]):
+        advance(time, wanted)
+        act()
+    assert not any(pending.values())
     rest[4].wait()
-    x_all.wait_send()
+    x_wait(lambda c: c.wait_send())
     q_all.wait_send()
     for d in range(1, tp):
         p_copy(d).wait_send()
-        xt_copy(d, mt).wait_send()
 
     def sent(d, pieces):
         all_of = W.at[:, pl.ds(0, pieces * depth // G), :]
@@ -446,23 +480,13 @@
             device_id={"sp": partner[X]}, device_id_type=pl.DeviceIdType.MESH,
         ).wait_send()
 
-    def plane_pieces(d, inner, outers):
-        turned = sum(s == d for s in second)
-        halves = 2 * sum(s == d and not w for s, w in zip(second, wide))
-        return (inner + 1) * (G + turned) + outers * halves
-
-    def settle(inner, outers):
-        for d in (X, Y):
-            sent(d, plane_pieces(d, inner, outers))
-
-    pl.when(outer)(lambda: settle(max(L - 2, 0), min(L - 1, 1)))
-    if L > 2:
-        pl.when(jnp.logical_not(outer))(lambda: settle(L - 3, 2))
-    total = 0
-    for k in range(L - 1):
-        total += G if 0 < k else 2 * G + 2 * len(wides)
-        pl.when(z == k)(lambda total=total: sent(UP, total))
-        pl.when(z == L - 1 - k)(lambda total=total: sent(DOWN, total))
+    def settle(k):
+        for d in range(4):
+            pieces = sum(link == d for _, link in plan.start[k])
+            if pieces:
+                sent(d, pieces // 2)
+
+    by_role(settle)
 
 
 def read(keys, values, mix, gain, k_out, v_out, read_out, sem):
@@ -511,8 +535,8 @@
             pltpu.VMEM((rows, tp * wl), BF16),
             pltpu.VMEM((G, rows, cols // G), F32),
             pltpu.VMEM((1, wl), BF16),
-            pltpu.VMEM((tp, n, 1, wl), F32),
-            pltpu.VMEM((n, wl), F32),
+            pltpu.VMEM((n, 1, max(depth, LANES)), BF16),
+            pltpu.VMEM((n, max(depth, LANES)), F32),
             pltpu.VMEM((depth, cols), BF16),
             pltpu.VMEM((n, 1, cols), F32),
             pltpu.VMEM((n, 1, cols), F32),
@@ -521,7 +545,7 @@
             pltpu.VMEM((2 * hp, cols), BF16),
             pltpu.VMEM((1, heads), F32),
             dma((2 * G * n,)), dma((4,)), dma((tp,)), dma((tp,)), dma((1,)), dma((1,)),
-            dma((tp,)), dma((tp,)), dma((1,)), dma((1,)), dma((7,)),
+            dma((1,)), dma((1,)), dma((7,)),
             pltpu.SemaphoreType.REGULAR((4,)),
         ],
         compiler_params=pltpu.CompilerParams(

time: 71.6 us -> 69.5 us (0.971)
  Pallas kernels: 70.8 us -> 68.7 us
    pallas_call x1, Pallas kernels: 68.2 us -> 66.1 us  [body(): pl.pallas_call(functools.partial(kernel, n, tp, G, heads), out_shape=(plt...]
where the time goes in v2:
time: 69.5 us; the launch traced here: 69.3 us
  Pallas kernels  68.7 us (99%)
    pallas_call x1, Pallas kernels, body(): pl.pallas_call(functools.partial(kernel, n, tp, G, heads), out_shape=(plt...  66.1 us
    pallas_call x1, Pallas kernels, body(): pl.pallas_call(read, out_shape=(jax.ShapeDtypeStruct((seqs, rows, cols),...  2.64 us

profile of v2, /device:TPU:0, one launch (start us, length us, event | category | flops | bytes accessed | tf_op | source)
XLA Modules:
  0.0 69.3 jit_solution(1008911473571026038)
XLA Ops:
  0.6 66.1 %prefill.1 = (bf16[1024,1024]{1,0:T(8,128)(2,1)S(1)}, bf16[1024,1024]{1,0:T(8,128)(2,1)S(1)}, bf16[24,1024]{1,0:T(8,128)(2,1)S(1)}, f32[1,128]{1,0:T(1,128)S(1)}) custom-call(bf16[1,1024,1024]{2,1,0:T(8,128)(2,1)} %prompt.1, bf16[1,1024]{1,0:T(2,128)(2,1)} %fresh.1, bf16[128,1024]{1,0:T(8,128)(2,1)} %wq.1, bf16[128,1024]{1,0:T(8,128)(2,1)} %wk.1, ...), custom_call_target="tpu_custom_call" | custom-call | tf_op jit(solution)/shard_map/prefill/pallas_call | solution.py:523
  66.7 2.6 %read.1 = (bf16[1,1024,1024]{2,1,0:T(8,128)(2,1)}, bf16[1,1024,1024]{2,1,0:T(8,128)(2,1)}, bf16[1,8,128]{2,1,0:T(8,128)(2,1)}) custom-call(bf16[1024,1024]{1,0:T(8,128)(2,1)S(1)} %get-tuple-element.7.keys, bf16[1024,1024]{1,0:T(8,128)(2,1)S(1)} %get-tuple-element.8.values, bf16[24,1024]{1,0:T(8,128)(2,1)S(1)} %get-tuple-element.9.mix, ...), custom_call_target="tpu_custom_call" | custom-call | tf_op jit(solution)/shard_map/read/pallas_call | solution.py:555

commit v3 on v2

--- a/solution.py
+++ b/solution.py
@@ -17,7 +17,7 @@
 
 X, Y, UP, DOWN = 0, 1, 2, 3
 LAG, LEAD = 0.9, 3.0
-TOK0, TOK1 = 2.5, 4.0
+TOKC, TOK0, TOK1 = 1.0, 2.5, 4.0
 F32, BF16 = jnp.float32, jnp.bfloat16
 
 
@@ -121,21 +121,40 @@
         own = ((max(self.arrival[k][p], t - LEAD), t, p, d) for (p, d), t in self.start[k].items())
         return [(when, p, d) for when, _, p, d in sorted(own)]
 
-    def pieces(self, m, zo, groups):
-        return [(m, j, zo, dy, dx) for j in groups for dy in range(2) for dx in range(2)]
-
-    def ready(self, k, m, zo, groups):
-        return max(self.arrival[k][p] for p in self.pieces(m, zo, groups))
+    def pieces(self, m, zo, groups, sides=(0, 1)):
+        return [(m, j, zo, dy, dx) for j in groups for dy in sides for dx in range(2)]
+
+    def ready(self, k, m, zo, groups, sides=(0, 1)):
+        return max(self.arrival[k][p] for p in self.pieces(m, zo, groups, sides))
 
     def order(self, k, m):
         everything = range(self.G)
         return sorted(range(self.L), key=lambda zo: (zo != k, self.ready(k, m, zo, everything)))
 
 
+def rows_of(zo, y, depth):
+    if 2 * depth % LANES:
+        return pl.ds(pl.multiple_of(zo * 4 * depth, 4 * depth), 4 * depth)
+    return pl.ds(pl.multiple_of((zo * 4 + y * 2) * depth, 2 * depth), 2 * depth)
+
+
+def ending(plan, z):
+    L, m = plan.L, 1
+    role = jnp.minimum(z, L - 1 - z)
+    ahead = jnp.where(z <= L - 1 - z, 1, -1)
+    zo, ready = z, {j: 0.0 for j in range(plan.G)}
+    for k in plan.roles():
+        final = plan.order(k, m)[-1]
+        zo = jnp.where(role == k, z + ahead * (final - k), zo)
+        for j in ready:
+            ready[j] = max(ready[j], plan.ready(k, m, final, [j]))
+    return role, ahead, zo, [j for j in ready if ready[j] > max(ready.values()) - 0.5]
+
+
 def kernel(
     n, tp, G, heads, prompt, fresh, wq, wk, wv, lam, gain,
-    k_out, v_out, mix_out, gain_out,
-    W, PR, acc, fr, XR, XM, wq_v, QS, QR, ct, st, qs, lam_v,
+    k_out, v_out, mix_out, gain_out, W, PR, acc,
+    fr, XR, XM, wq_v, QS, QR, ct, st, qs, lam_v,
     w_recv, w_send, p_recv, p_send, x_recv, x_send, q_recv, q_send, loc, token,
 ):
     _, rows, wl = prompt.shape
@@ -150,8 +169,7 @@
     outer = jnp.logical_not(up_ok & down_ok)
 
     plan = Plan(L, G)
-    role = jnp.minimum(z, L - 1 - z)
-    ahead = jnp.where(z <= L - 1 - z, 1, -1)
+    role, ahead, last_plane, late = ending(plan, z)
 
     def at(zo, yo, xo):
         return zo * 4 + yo * 2 + xo
@@ -202,21 +220,24 @@
     def loop(lo, hi, f):
         lax.fori_loop(lo, hi, lambda i, _: (f(i), _)[1], 0)
 
-    R = min(rows, 512)
-
     turns = {(k, m): plan.order(k, m) for k in plan.roles() for m in range(2)}
 
-    def dots(m, t, groups=range(G), last=False):
+    def dots(m, t, groups=range(G), sides=(0, 1), last=False):
         zo = z
         for k in plan.roles():
             zo = jnp.where(role == k, z + ahead * (turns[k, m][t] - k), zo)
 
+        R = rows // len(sides)
+
         def tile(i):
             r = pl.ds(pl.multiple_of(i * R, R), R)
-            p = pl.ds(pl.multiple_of(zo * plane, plane), plane)
+            if len(sides) == 2:
+                p = pl.ds(pl.multiple_of(zo * plane, plane), plane)
+            else:
+                p = rows_of(zo, yf if sides[0] else y, depth)
             for j in groups:
                 part = jnp.dot(PR[r, p], W[m * G + j, p, :], preferred_element_type=F32)
-                if t > 0:
+                if t > 0 or sides == (1,):
                     part = acc[j, r, :] + part
                 if last:
                     v_out[r, pl.ds(j * width, width)] = part.astype(BF16)
@@ -226,9 +247,14 @@
         loop(0, rows // R, tile)
 
     barrier = pltpu.get_barrier_semaphore()
-    for d in range(1, tp):
-        pl.semaphore_signal(
-            barrier, inc=1, device_id={"tp": (mt + d) % tp}, device_id_type=pl.DeviceIdType.MESH)
+
+    def cores(which, sem):
+        for t in range(tp):
+            @pl.when(t > mt if which > 0 else t < mt)
+            def _(t=t):
+                pl.semaphore_signal(sem, inc=1, device_id={"tp": t}, device_id_type=pl.DeviceIdType.MESH)
+
+    cores(1, barrier)
 
     def signal(sem, d):
         pl.semaphore_signal(
@@ -266,14 +292,7 @@
         c.start()
     own_wait(0)
 
-    @pl.when(up_ok & down_ok)
-    def _():
-        pl.semaphore_wait(barrier, 4 + tp - 1)
-
-    @pl.when(outer)
-    def _():
-        pl.semaphore_wait(barrier, 3 + tp - 1)
-
+    pl.semaphore_wait(barrier, 2 + up_ok.astype(jnp.int32) + down_ok.astype(jnp.int32) + mt)
 
     block_of = XR.shape[2]
     share = wl // depth
@@ -329,7 +348,7 @@
         )
 
     advance(0.0001)
-    signal(token.at[Y], Y)
+    cores(-1, token.at[4])
 
     def relay_token(b):
         for turn, before, more, d in ((z == b, down_ok, up_ok, UP), (z == L - 1 - b, up_ok, down_ok, DOWN)):
@@ -338,8 +357,6 @@
 
     rest[0].wait()
     own_wait(1)
-    for d in range(1, tp):
-        p_copy(d).start()
 
 
     def q_copy(d):
@@ -416,14 +433,26 @@
         low = (left - mid.astype(F32)).astype(BF16)
         mix_out[...] = jnp.concatenate([high, mid, low], axis=0)
 
-    def when_ready(m, t, groups):
-        return max(plan.ready(k, m, turns[k, m][t], groups) for k in plan.roles())
+    def when_ready(m, t, groups, sides=(0, 1)):
+        return max(plan.ready(k, m, turns[k, m][t], groups, sides) for k in plan.roles())
+
+    def add_dots(when, m, t, groups=range(G), sides=(0, 1), last=False):
+        def wanted(k):
+            return plan.pieces(m, turns[k, m][t], groups, sides)
+
+        work.append((when, functools.partial(dots, m, t, groups, sides, last), wanted))
 
     def prompt_whole():
         rest[1].wait()
         for d in range(1, tp):
             p_wait(d).wait_recv()
 
+    def all_cores():
+        pl.when(mt < tp - 1)(lambda: pl.semaphore_wait(token.at[4], tp - 1 - mt))
+        signal(token.at[Y], Y)
+        for d in range(1, tp):
+            p_copy(d).start()
+
     def first_token():
         pl.semaphore_wait(token.at[Y], 1)
         signal(token.at[X], X)
@@ -437,7 +466,7 @@
 
     none = lambda k: ()
     work = [
-        (TOK0, first_token, none), (TOK1, second_token, none),
+        (TOKC, all_cores, none), (TOK0, first_token, none), (TOK1, second_token, none),
         *((TOK1 + 0.9 * b, functools.partial(relay_token, b), none) for b in range(1, L)),
     ]
     sent_x = TOK1 + 0.9 * L
@@ -447,17 +476,30 @@
     keys_at = 0
     for m in range(2):
         for t in range(L):
-            last = m == 1 and t == L - 1
-            when = when_ready(m, t, range(G)) + 0.1
-            if m == 0 and t == 0:
-                work.append((when, prompt_whole, none))
-            if m == 1 and t == 0:
-                when = max(when, keys_at + 2.5)
+            when = when_ready(m, t, range(G)) + 0.1 + 0.001 * t
             if m == 0:
                 keys_at = max(keys_at, when)
-            work.append((
-                when + 0.001 * t, functools.partial(dots, m, t, last=last),
-                lambda k, m=m, t=t: plan.pieces(m, turns[k, m][t], range(G))))
+            if (m, t) == (0, 0):
+                work.append((when - 0.01, prompt_whole, none))
+            if (m, t) == (1, 0):
+                when = max(when, keys_at + 2.5)
+            if m == 0 or t < max(L - 2, 1):
+                add_dots(when, m, t)
+                continue
+            last, after = t == L - 1, 0
+            for sides in ([(0,), (1,)] if 2 * depth % LANES == 0 else [(0, 1)]):
+                ready = {j: when_ready(m, t, [j], sides) for j in range(G)}
+                if not last:
+                    parts = [list(range(G))]
+                elif sides == (0,):
+                    edge = max(ready.values()) - 3
+                    parts = [[j for j in ready if ready[j] < edge], [j for j in ready if ready[j] >= edge]]
+                else:
+                    parts = [[j for j in ready if j not in late]]
+                for some in parts:
+                    if some:
+                        after = max(after, max(ready[j] for j in some)) + 0.02
+                        add_dots(after + 0.01 * t, m, t, some, sides, last and 1 in sides)
     work.append((keys_at + 0.1, lambda: turn_rows(0), none))
     work.append((keys_at + 1.3, lambda: turn_rows(1), none))
     answer = max(sent_x + 9 + 12, keys_at + 2.4)
@@ -466,7 +508,7 @@
     for time, act, wanted in sorted(work, key=lambda item: item[0]):
         advance(time, wanted)
         act()
-    assert not any(pending.values())
+    advance(2 * plan.end, lambda k: plan.pieces(1, turns[k, 1][L - 1], late))
     rest[4].wait()
     x_wait(lambda c: c.wait_send())
     q_all.wait_send()
@@ -489,20 +531,40 @@
     by_role(settle)
 
 
-def read(keys, values, mix, gain, k_out, v_out, read_out, sem):
+def read(n, G, keys, values, mix, gain, W, PR, acc, k_out, v_out, read_out, fresh, sem):
     hp = mix.shape[0] // 3
     heads = read_out.shape[1]
+    depth, width = W.shape[1] // n, W.shape[2]
+    me = lax.axis_index("sp")
+    _, _, zo, late = ending(Plan(n // 4, G), me // 4)
     k_copy = pltpu.make_async_copy(keys, k_out.at[0], sem.at[0])
-    v_copy = pltpu.make_async_copy(values, v_out.at[0], sem.at[1])
-    v_copy.start()
     k_copy.start()
-    mixed = jnp.dot(mix[...], values[...], preferred_element_type=F32)
+
+    def columns(j):
+        return pl.ds(j * width, width)
+
+    source = [fresh if j in late else values for j in range(G)]
+    v_copies = [
+        pltpu.make_async_copy(source[j].at[:, columns(j)], v_out.at[0, :, columns(j)], sem.at[1 + j])
+        for j in range(G)
+    ]
+    for j in range(G):
+        if j not in late:
+            v_copies[j].start()
+    p = rows_of(zo, 1 - (me // 2) % 2, depth)
+    for j in late:
+        part = acc[j] + jnp.dot(PR[:, p], W[G + j, p, :], preferred_element_type=F32)
+        fresh[:, columns(j)] = part.astype(BF16)
+        v_copies[j].start()
+    mixed = jnp.concatenate(
+        [jnp.dot(mix[...], source[j][:, columns(j)], preferred_element_type=F32) for j in range(G)], axis=1)
     mixed = mixed[:hp] + mixed[hp:2 * hp] + mixed[2 * hp:]
     diff = jnp.concatenate(
         [mixed[h:h + 1, h * VAL_DIM:(h + 1) * VAL_DIM] for h in range(heads)], axis=0)
     normed = diff * lax.rsqrt(jnp.mean(diff * diff, axis=-1, keepdims=True) + norm_eps)
     read_out[0] = (normed * gain[...]).astype(BF16)
-    v_copy.wait()
+    for c in v_copies:
+        c.wait()
     k_copy.wait()
 
 
@@ -520,20 +582,20 @@
     hbm = pl.BlockSpec(memory_space=pltpu.HBM)
     vmem = pl.BlockSpec(memory_space=pltpu.VMEM)
     dma = pltpu.SemaphoreType.DMA
-    keys, values, mix, gain = pl.pallas_call(
+    keys, values, *passed = pl.pallas_call(
         functools.partial(kernel, n, tp, G, heads),
         out_shape=(
             pltpu.VMEM((rows, cols), BF16),
             pltpu.VMEM((rows, cols), BF16),
             pltpu.VMEM((3 * hp, rows), BF16),
             pltpu.VMEM((1, VAL_DIM), F32),
-        ),
-        in_specs=[hbm] * 7,
-        out_specs=(vmem, vmem, vmem, vmem),
-        scratch_shapes=[
             pltpu.VMEM((2 * G, n * depth, cols // G), BF16),
             pltpu.VMEM((rows, tp * wl), BF16),
             pltpu.VMEM((G, rows, cols // G), F32),
+        ),
+        in_specs=[hbm] * 7,
+        out_specs=(vmem,) * 7,
+        scratch_shapes=[
             pltpu.VMEM((1, wl), BF16),
             pltpu.VMEM((n, 1, max(depth, LANES)), BF16),
             pltpu.VMEM((n, max(depth, LANES)), F32),
@@ -546,25 +608,25 @@
             pltpu.VMEM((1, heads), F32),
             dma((2 * G * n,)), dma((4,)), dma((tp,)), dma((tp,)), dma((1,)), dma((1,)),
             dma((1,)), dma((1,)), dma((7,)),
-            pltpu.SemaphoreType.REGULAR((4,)),
+            pltpu.SemaphoreType.REGULAR((5,)),
         ],
         compiler_params=pltpu.CompilerParams(
-            collective_id=0, has_side_effects=True, vmem_limit_bytes=44 * 1024 * 1024),
+            collective_id=0, has_side_effects=True, vmem_limit_bytes=20 * 1024 * 1024),
         name="prefill",
     )(*operands)
     return pl.pallas_call(
-        read,
+        functools.partial(read, n, G),
         out_shape=(
             jax.ShapeDtypeStruct((seqs, rows, cols), BF16),
             jax.ShapeDtypeStruct((seqs, rows, cols), BF16),
             jax.ShapeDtypeStruct((seqs, heads, VAL_DIM), BF16),
         ),
-        in_specs=[vmem] * 4,
+        in_specs=[vmem] * 7,
         out_specs=(any_, any_, vmem),
-        scratch_shapes=[dma((2,))],
+        scratch_shapes=[pltpu.VMEM((rows, cols), BF16), dma((1 + G,))],
         compiler_params=pltpu.CompilerParams(vmem_limit_bytes=24 * 1024 * 1024),
         name="read",
-    )(keys, values, mix, gain)
+    )(keys, values, *passed)
 
 
 def solution(mesh):

time: 69.5 us -> 68.4 us (0.984)
  Pallas kernels: 68.7 us -> 67.6 us
    pallas_call x1, Pallas kernels: 66.1 us -> 64.7 us  [body(): pl.pallas_call(functools.partial(kernel, n, tp, G, heads), out_shape=(plt...]
where the time goes in v3:
time: 68.4 us; the launch traced here: 68.3 us
  Pallas kernels  67.6 us (99%)
    pallas_call x1, Pallas kernels, body(): pl.pallas_call(functools.partial(kernel, n, tp, G, heads), out_shape=(plt...  64.7 us
    pallas_call x1, Pallas kernels, body(): pl.pallas_call(functools.partial(read, n, G), out_shape=(jax.ShapeDtypeSt...  2.91 us

profile of v3, /device:TPU:0, one launch (start us, length us, event | category | flops | bytes accessed | tf_op | source)
XLA Modules:
  0.0 68.3 jit_solution(8328381248144186448)
XLA Ops:
  0.6 64.7 %prefill.1 = (bf16[1024,1024]{1,0:T(8,128)(2,1)S(1)}, bf16[1024,1024]{1,0:T(8,128)(2,1)S(1)}, bf16[24,1024]{1,0:T(8,128)(2,1)S(1)}, f32[1,128]{1,0:T(1,128)S(1)}...) custom-call(bf16[1,1024,1024]{2,1,0:T(8,128)(2,1)} %prompt.1, ...), custom_call_target="tpu_custom_call" | custom-call | tf_op jit(solution)/shard_map/prefill/pallas_call | solution.py:585
  65.4 2.9 %read.1 = (bf16[1,1024,1024]{2,1,0:T(8,128)(2,1)}, bf16[1,1024,1024]{2,1,0:T(8,128)(2,1)}, bf16[1,8,128]{2,1,0:T(8,128)(2,1)}) custom-call(bf16[1024,1024]{1,0:T(8,128)(2,1)S(1)} %get-tuple-element.10.keys, bf16[1024,1024]{1,0:T(8,128)(2,1)S(1)} %get-tuple-element.11.values, bf16[24,1024]{1,0:T(8,128)(2,1)S(1)} %get-tuple-element.12.mix, ...), custom_call_target="tpu_custom_call" | custom-call | tf_op jit(solution)/shard_map/read/pallas_call | solution.py:617

commit v4 on v3

--- a/solution.py
+++ b/solution.py
@@ -16,7 +16,7 @@
 norm_eps = 1e-05
 
 X, Y, UP, DOWN = 0, 1, 2, 3
-LAG, LEAD = 0.9, 3.0
+LAG, LEAD = 0.9, 2.0
 TOKC, TOK0, TOK1 = 1.0, 2.5, 4.0
 F32, BF16 = jnp.float32, jnp.bfloat16
 
@@ -50,7 +50,7 @@
         self.first = [X if j < (G + 1) // 2 else Y for j in range(G)]
         self.wide = [G >= 4 and j % 2 == 1 for j in range(G)]
         self.arrival = [{} for _ in range(L)]
-        self.start = [{} for _ in range(L)]
+        self.issue = [{} for _ in range(L)]
         waiting = {(z, d): [] for z in range(L) for d in range(4)}
         free = dict.fromkeys(waiting, 0.0)
         events, count = [], 0
@@ -61,12 +61,13 @@
             heapq.heappush(events, (time, count, what))
 
         def begin(z, d, time):
-            if waiting[z, d] and free[z, d] <= time:
+            while waiting[z, d] and free[z, d] - time < LEAD - 0.01:
                 piece = heapq.heappop(waiting[z, d])[-1]
-                self.start[z][piece, d] = time
-                free[z, d] = time + 1
-                post(time + 1, (z, d, None))
-                post(time + 1 + LAG, (*self.beyond(z, piece, d)[:1], None, self.beyond(z, piece, d)[1]))
+                self.issue[z][piece, d] = time
+                free[z, d] = max(time, free[z, d]) + 1
+                there, seen = self.beyond(z, piece, d)
+                post(free[z, d] + LAG, (there, None, seen))
+                post(max(time, free[z, d] - LEAD + 0.02), (z, d, None))
 
         for z in range(L):
             for m in range(2):
@@ -118,8 +119,8 @@
         return range((self.L + 1) // 2)
 
     def sends(self, k):
-        own = ((max(self.arrival[k][p], t - LEAD), t, p, d) for (p, d), t in self.start[k].items())
-        return [(when, p, d) for when, _, p, d in sorted(own)]
+        return [(when, p, d) for when, _, (p, d) in sorted(
+            (when, i, send) for i, (send, when) in enumerate(self.issue[k].items()))]
 
     def pieces(self, m, zo, groups, sides=(0, 1)):
         return [(m, j, zo, dy, dx) for j in groups for dy in sides for dx in range(2)]
@@ -154,8 +155,8 @@
 def kernel(
     n, tp, G, heads, prompt, fresh, wq, wk, wv, lam, gain,
     k_out, v_out, mix_out, gain_out, W, PR, acc,
-    fr, XR, XM, wq_v, QS, QR, ct, st, qs, lam_v,
-    w_recv, w_send, p_recv, p_send, x_recv, x_send, q_recv, q_send, loc, token,
+    fr, XR, XM, wq_v, QS, QP, QT, QR, ct, st, qs, lam_v,
+    w_recv, w_send, p_recv, p_send, x_recv, x_send, q_recv, q_send, t_recv, t_send, loc, token,
 ):
     _, rows, wl = prompt.shape
     depth, cols = wk.shape
@@ -330,7 +331,8 @@
         pl.when(mine)(lambda: end(together(XR.at[pl.ds(0, n - 1)], x_send, x_recv)))
         pl.when(jnp.logical_not(mine))(lambda: end(together(XR, x_send, x_recv)))
 
-    q_all = together(QR.at[pl.ds(0, n - 1)], q_send, q_recv)
+    q_all = together(QP.at[pl.ds(0, 3)], q_send, q_recv)
+    t_all = together(QR.at[pl.ds(0, L - 1)], t_send, t_recv) if L > 1 else None
 
     def p_copy(d):
         return pltpu.make_async_remote_copy(
@@ -359,12 +361,22 @@
     own_wait(1)
 
 
+    spot = me % 4
+
     def q_copy(d):
-        dst = (me + d) % n
+        other = (spot + d) % 4
         return pltpu.make_async_remote_copy(
-            src_ref=QS.at[dst], dst_ref=QR.at[me],
+            src_ref=QS.at[other], dst_ref=QP.at[spot],
             send_sem=q_send.at[0], recv_sem=q_recv.at[0],
-            device_id={"sp": dst}, device_id_type=pl.DeviceIdType.MESH,
+            device_id={"sp": z * 4 + other}, device_id_type=pl.DeviceIdType.MESH,
+        )
+
+    def t_copy(d):
+        other = (z + d) % L
+        return pltpu.make_async_remote_copy(
+            src_ref=QT.at[other], dst_ref=QR.at[z],
+            send_sem=t_send.at[0], recv_sem=t_recv.at[0],
+            device_id={"sp": other * 4 + spot}, device_id_type=pl.DeviceIdType.MESH,
         )
 
     def partial_queries():
@@ -382,18 +394,26 @@
         rest[2].wait()
         partial = jnp.dot(chosen, wq_v[...], preferred_element_type=F32)
         for j in range(n):
-            QS[j] = partial[j:j + 1, :]
-        QR[me] = QS[me]
-        loop(1, n, lambda d: q_copy(d).start())
+            QS[j % 4, j // 4] = partial[j:j + 1, :]
+        QP[spot] = QS[spot]
+        loop(1, 4, lambda d: q_copy(d).start())
+
+    def plane_queries():
+        q_all.wait_recv()
+        QT[...] = (QP[0] + QP[1]) + (QP[2] + QP[3])
+        QR[z] = QT[z]
+        if L > 1:
+            loop(1, L, lambda d: t_copy(d).start())
 
     hp = max(heads, 8)
     pad = 2 * hp
 
     def build_query():
         qcos, qsin = table(jnp.full((8, LANES), rows, F32))
-        q_all.wait_recv()
+        if L > 1:
+            t_all.wait_recv()
         total = QR[0]
-        for j in range(1, n):
+        for j in range(1, L):
             total = total + QR[j]
         total = jnp.broadcast_to(total, (8, cols))
         query = jnp.concatenate(
@@ -475,6 +495,7 @@
     work.append((sent_x + 4, lambda: loop(0, rows // 64, angles), none))
     keys_at = 0
     for m in range(2):
+        whole_until = split_until = 0
         for t in range(L):
             when = when_ready(m, t, range(G)) + 0.1 + 0.001 * t
             if m == 0:
@@ -483,10 +504,13 @@
                 work.append((when - 0.01, prompt_whole, none))
             if (m, t) == (1, 0):
                 when = max(when, keys_at + 2.5)
-            if m == 0 or t < max(L - 2, 1):
+            when = max(when, whole_until + 0.01)
+            if m == 0 or t < max(L - 2, min(1, L - 1)):
+                whole_until = when
+                keys_at = max(keys_at, when) if m == 0 else keys_at
                 add_dots(when, m, t)
                 continue
-            last, after = t == L - 1, 0
+            last, after = t == L - 1, whole_until
             for sides in ([(0,), (1,)] if 2 * depth % LANES == 0 else [(0, 1)]):
                 ready = {j: when_ready(m, t, [j], sides) for j in range(G)}
                 if not last:
@@ -498,11 +522,14 @@
                     parts = [[j for j in ready if j not in late]]
                 for some in parts:
                     if some:
-                        after = max(after, max(ready[j] for j in some)) + 0.02
-                        add_dots(after + 0.01 * t, m, t, some, sides, last and 1 in sides)
+                        ends = last and 1 in sides
+                        after = max(after, max(ready[j] for j in some), split_until if ends else 0) + 0.02
+                        split_until = max(split_until, after)
+                        add_dots(after, m, t, some, sides, ends)
     work.append((keys_at + 0.1, lambda: turn_rows(0), none))
     work.append((keys_at + 1.3, lambda: turn_rows(1), none))
-    answer = max(sent_x + 9 + 12, keys_at + 2.4)
+    work.append((sent_x + 17, plane_queries, none))
+    answer = max(sent_x + 17 + 9, keys_at + 2.4)
     work.append((answer, build_query, none))
     work.append((answer + 0.5, weigh, none))
     for time, act, wanted in sorted(work, key=lambda item: item[0]):
@@ -512,6 +539,8 @@
     rest[4].wait()
     x_wait(lambda c: c.wait_send())
     q_all.wait_send()
+    if L > 1:
+        t_all.wait_send()
     for d in range(1, tp):
         p_copy(d).wait_send()
 
@@ -524,7 +553,7 @@
 
     def settle(k):
         for d in range(4):
-            pieces = sum(link == d for _, link in plan.start[k])
+            pieces = sum(link == d for _, link in plan.issue[k])
             if pieces:
                 sent(d, pieces // 2)
 
@@ -600,14 +629,16 @@
             pltpu.VMEM((n, 1, max(depth, LANES)), BF16),
             pltpu.VMEM((n, max(depth, LANES)), F32),
             pltpu.VMEM((depth, cols), BF16),
-            pltpu.VMEM((n, 1, cols), F32),
-            pltpu.VMEM((n, 1, cols), F32),
+            pltpu.VMEM((4, n // 4, 1, cols), F32),
+            pltpu.VMEM((4, n // 4, 1, cols), F32),
+            pltpu.VMEM((n // 4, 1, cols), F32),
+            pltpu.VMEM((n // 4, 1, cols), F32),
             pltpu.VMEM((rows, LANES), F32),
             pltpu.VMEM((rows, LANES), F32),
             pltpu.VMEM((2 * hp, cols), BF16),
             pltpu.VMEM((1, heads), F32),
             dma((2 * G * n,)), dma((4,)), dma((tp,)), dma((tp,)), dma((1,)), dma((1,)),
-            dma((1,)), dma((1,)), dma((7,)),
+            dma((1,)), dma((1,)), dma((1,)), dma((1,)), dma((7,)),
             pltpu.SemaphoreType.REGULAR((5,)),
         ],
         compiler_params=pltpu.CompilerParams(

time: 68.4 us -> 67.4 us (0.985)
  Pallas kernels: 67.6 us -> 66.6 us
    pallas_call x1, Pallas kernels: 64.7 us -> 63.9 us  [body(): pl.pallas_call(functools.partial(kernel, n, tp, G, heads), out_shape=(plt...]
where the time goes in v4:
time: 67.4 us; the launch traced here: 67.2 us
  Pallas kernels  66.6 us (99%)
    pallas_call x1, Pallas kernels, body(): pl.pallas_call(functools.partial(kernel, n, tp, G, heads), out_shape=(plt...  63.9 us
    pallas_call x1, Pallas kernels, body(): pl.pallas_call(functools.partial(read, n, G), out_shape=(jax.ShapeDtypeSt...  2.66 us

profile of v4, /device:TPU:0, one launch (start us, length us, event | category | flops | bytes accessed | tf_op | source)
XLA Modules:
  0.0 67.2 jit_solution(1229583909143698371)
XLA Ops:
  0.6 63.9 %prefill.1 = (bf16[1024,1024]{1,0:T(8,128)(2,1)S(1)}, bf16[1024,1024]{1,0:T(8,128)(2,1)S(1)}, bf16[24,1024]{1,0:T(8,128)(2,1)S(1)}, f32[1,128]{1,0:T(1,128)S(1)}...) custom-call(bf16[1,1024,1024]{2,1,0:T(8,128)(2,1)} %prompt.1, ...), custom_call_target="tpu_custom_call" | custom-call | tf_op jit(solution)/shard_map/prefill/pallas_call | solution.py:614
  64.6 2.7 %read.1 = (bf16[1,1024,1024]{2,1,0:T(8,128)(2,1)}, bf16[1,1024,1024]{2,1,0:T(8,128)(2,1)}, bf16[1,8,128]{2,1,0:T(8,128)(2,1)}) custom-call(bf16[1024,1024]{1,0:T(8,128)(2,1)S(1)} %get-tuple-element.10.keys, bf16[1024,1024]{1,0:T(8,128)(2,1)S(1)} %get-tuple-element.11.values, bf16[24,1024]{1,0:T(8,128)(2,1)S(1)} %get-tuple-element.12.mix, ...), custom_call_target="tpu_custom_call" | custom-call | tf_op jit(solution)/shard_map/read/pallas_call | solution.py:648

commit v5 on v4

--- a/solution.py
+++ b/solution.py
@@ -560,7 +560,7 @@
     by_role(settle)
 
 
-def read(n, G, keys, values, mix, gain, W, PR, acc, k_out, v_out, read_out, fresh, sem):
+def read(n, G, keys, values, mix, gain, W, PR, acc, k_out, v_out, read_out, fresh, answer, sem):
     hp = mix.shape[0] // 3
     heads = read_out.shape[1]
     depth, width = W.shape[1] // n, W.shape[2]
@@ -591,10 +591,13 @@
     diff = jnp.concatenate(
         [mixed[h:h + 1, h * VAL_DIM:(h + 1) * VAL_DIM] for h in range(heads)], axis=0)
     normed = diff * lax.rsqrt(jnp.mean(diff * diff, axis=-1, keepdims=True) + norm_eps)
-    read_out[0] = (normed * gain[...]).astype(BF16)
+    answer[0] = (normed * gain[...]).astype(BF16)
+    r_copy = pltpu.make_async_copy(answer, read_out, sem.at[1 + G])
+    r_copy.start()
     for c in v_copies:
         c.wait()
     k_copy.wait()
+    r_copy.wait()
 
 
 def body(n, tp, prompt, new_input, w_query, w_key, w_value, lam, out_gain):
@@ -653,8 +656,9 @@
             jax.ShapeDtypeStruct((seqs, heads, VAL_DIM), BF16),
         ),
         in_specs=[vmem] * 7,
-        out_specs=(any_, any_, vmem),
-        scratch_shapes=[pltpu.VMEM((rows, cols), BF16), dma((1 + G,))],
+        out_specs=(any_, any_, any_),
+        scratch_shapes=[
+            pltpu.VMEM((rows, cols), BF16), pltpu.VMEM((1, heads, VAL_DIM), BF16), dma((2 + G,))],
         compiler_params=pltpu.CompilerParams(vmem_limit_bytes=24 * 1024 * 1024),
         name="read",
     )(keys, values, *passed)

time: 67.4 us -> 66.8 us (level)
  no operation moved by 1% of the time
where the time goes in v5:
time: 66.8 us; the launch traced here: 66.7 us
  Pallas kernels  66 us (99%)
    pallas_call x1, Pallas kernels, body(): pl.pallas_call(functools.partial(kernel, n, tp, G, heads), out_shape=(plt...  63.9 us
    pallas_call x1, Pallas kernels, body(): pl.pallas_call(functools.partial(read, n, G), out_shape=(jax.ShapeDtypeSt...  2.1 us

profile of v5, /device:TPU:0, one launch (start us, length us, event | category | flops | bytes accessed | tf_op | source)
XLA Modules:
  0.0 66.7 jit_solution(9232889513730767629)
XLA Ops:
  0.6 63.9 %prefill.1 = (bf16[1024,1024]{1,0:T(8,128)(2,1)S(1)}, bf16[1024,1024]{1,0:T(8,128)(2,1)S(1)}, bf16[24,1024]{1,0:T(8,128)(2,1)S(1)}, f32[1,128]{1,0:T(1,128)S(1)}...) custom-call(bf16[1,1024,1024]{2,1,0:T(8,128)(2,1)} %prompt.1, ...), custom_call_target="tpu_custom_call" | custom-call | tf_op jit(solution)/shard_map/prefill/pallas_call | solution.py:617
  64.6 2.1 %read.1 = (bf16[1,1024,1024]{2,1,0:T(8,128)(2,1)}, bf16[1,1024,1024]{2,1,0:T(8,128)(2,1)}, bf16[1,8,128]{2,1,0:T(8,128)(2,1)}) custom-call(bf16[1024,1024]{1,0:T(8,128)(2,1)S(1)} %get-tuple-element.10.keys, bf16[1024,1024]{1,0:T(8,128)(2,1)S(1)} %get-tuple-element.11.values, bf16[24,1024]{1,0:T(8,128)(2,1)S(1)} %get-tuple-element.12.mix, ...), custom_call_target="tpu_custom_call" | custom-call | tf_op jit(solution)/shard_map/read/pallas_call | solution.py:651
